TPU v7x, 256 devices: a whole 4x4x8 slice. The times are simulated.
256 devices in a mesh: ep: 64 (over z, x, core), tp: 4 (over y).
Axes of the slice: x: 4, y: 4, z: 8, core: 2. Of those that a mesh axis runs over, the one named last changes fastest.
Arguments:
- projected_queries: bfloat16 [16384, 2048], P('ep', 'tp'), may hold values from -245 to 245, as said below
- key_proj: bfloat16 [16384, 512], P('ep', 'tp'), may hold values from -6.2 to 6.2
- projected_values: bfloat16 [16384, 512], P('ep', 'tp'), may hold values from -24 to 24
- head_sink_logits: float32 [32], P('tp'), may hold values from 1 to 6
- out_weight: bfloat16 [2048, 4096], P('tp'), may hold values from -0.125 to 0.125
- expert_input: bfloat16 [8192, 4096], P('ep'), may hold values from -6 to 6
- norm_gain: float32 [4096], replicated, may hold values from 0.1 to 1.9
- routing: int32 [8192, 4], P('ep'), may hold values from 0 to 63, all different within a row; in each aligned block of 128 rows (0 to 127, 128 to 255, ...) at most 12 rows name the same one
- route_weight: float32 [8192, 4], P('ep'), may hold values from 0.1 to 1
- gate_weight: bfloat16 [64, 4096, 1024], P('ep', None, 'tp'), may hold values from -0.27929688 to 0.27929688
- up_weight: bfloat16 [64, 4096, 1024], P('ep', None, 'tp'), may hold values from -0.27929688 to 0.27929688
- down_weight: bfloat16 [64, 1024, 4096], P('ep', 'tp'), may hold values from -0.046875 to 0.046875
Outputs:
- mixer_output: bfloat16 [16384, 4096], P(('ep', 'tp'))
- expert_output: bfloat16 [8192, 4096], P('ep', 'tp')
Inputs may be any that keep to these rules, and one draw needn't show every extreme that they name: `projected_queries`: in the hidden draw some queries nearly equal a large multiple of a nearby key. `routing`: each row names 4 different experts; among the rows of one device (aligned blocks of 128 rows) no expert is named more than 12 times, a bound that some block reaches.
All inputs are finite; a program needn't handle non-finite values.
Results may differ from a plain program's by a relative error of at most 0.014.
Values may be sent and summed in bfloat16 or wider, within the bound.
No kernel may reach another device: no remote copies, remote signals or barrier semaphores. Data moves between devices by JAX's collectives and lax.ppermute only.
A program may use at most 128 MiB of HBM per device.

v0:
```python
import jax
import jax.numpy as jnp
from jax import lax
from jax.experimental import pallas as pl
from jax.experimental.pallas import tpu as pltpu
from jax.sharding import PartitionSpec as P

D = 4096
HEAD_SIZE = 64
WINDOW_KEYS = 128
TOPK = 4
EPS = 1e-06
CLAMP = 7.0
SLOPE = 1.702
N_TP = 4
SLOTS = 6
LANES = 256
BLOCKS = 3


def shifted(block, distance):
    return lax.ppermute(block, "tp", [((i + distance) % N_TP, i) for i in range(N_TP)])


def exchanged(block):
    return lax.all_to_all(block, "ep", split_axis=0, concat_axis=0, tiled=True)


def dot(a, b):
    return jnp.dot(a, b, preferred_element_type=jnp.float32)


def attention(projected_queries, key_proj, projected_values, head_sink_logits):
    query_rows = projected_queries.shape[0]
    kv_heads = key_proj.shape[1] // HEAD_SIZE
    heads_per_group = projected_queries.shape[1] // HEAD_SIZE // kv_heads
    count_of_blocks = query_rows // WINDOW_KEYS
    kept = key_proj.shape[1]
    prior = lax.ppermute(
        jnp.concatenate(
            [key_proj[query_rows - WINDOW_KEYS :], projected_values[query_rows - WINDOW_KEYS :]],
            axis=1,
        ),
        "ep",
        [(i, i + 1) for i in range(lax.axis_size("ep") - 1)],
    )
    prior_key, prior_value = prior[:, :kept], prior[:, kept:]
    key_all = jnp.concatenate([prior_key, key_proj], axis=0)
    value_all = jnp.concatenate([prior_value, projected_values], axis=0)
    window_keys = jnp.concatenate(
        [
            key_all[:-WINDOW_KEYS].reshape(count_of_blocks, WINDOW_KEYS, kv_heads, HEAD_SIZE),
            key_all[WINDOW_KEYS:].reshape(count_of_blocks, WINDOW_KEYS, kv_heads, HEAD_SIZE),
        ],
        axis=1,
    )
    window_values = jnp.concatenate(
        [
            value_all[:-WINDOW_KEYS].reshape(count_of_blocks, WINDOW_KEYS, kv_heads, HEAD_SIZE),
            value_all[WINDOW_KEYS:].reshape(count_of_blocks, WINDOW_KEYS, kv_heads, HEAD_SIZE),
        ],
        axis=1,
    )
    query_blocks = projected_queries.reshape(
        count_of_blocks, WINDOW_KEYS, kv_heads, heads_per_group, HEAD_SIZE
    )
    scores = jnp.einsum(
        "nqhgd,nshd->nhgqs", query_blocks, window_keys, preferred_element_type=jnp.float32
    ) * HEAD_SIZE ** (-0.5)
    offset = lax.axis_index("ep") * query_rows
    block_ids = jnp.arange(count_of_blocks)[:, None, None] * WINDOW_KEYS + offset
    query_pos = block_ids + jnp.arange(WINDOW_KEYS)[None, :, None]
    key_pos = block_ids - WINDOW_KEYS + jnp.arange(2 * WINDOW_KEYS)[None, None, :]
    permitted_mask = (key_pos <= query_pos) & (query_pos - key_pos < WINDOW_KEYS) & (key_pos >= 0)
    scores = jnp.where(permitted_mask[:, None, None, :, :], scores, -jnp.inf)
    sink_col = head_sink_logits.reshape(kv_heads, heads_per_group)[None, :, :, None, None]
    highest = jnp.maximum(jnp.max(scores, axis=-1, keepdims=True), sink_col)
    numerator = jnp.exp(scores - highest)
    denominator = jnp.sum(numerator, axis=-1, keepdims=True) + jnp.exp(sink_col - highest)
    weights = (numerator / denominator).astype(jnp.bfloat16)
    attended = jnp.einsum(
        "nhgqs,nshd->nqhgd", weights, window_values, preferred_element_type=jnp.float32
    )
    return attended.astype(jnp.bfloat16).reshape(
        query_rows, kv_heads * heads_per_group * HEAD_SIZE
    )


def params(mib):
    return pltpu.CompilerParams(vmem_limit_bytes=mib << 20)


def cost(flops, size):
    return pl.CostEstimate(flops=flops, bytes_accessed=size, transcendentals=0)


def dispatch_kernel(chunk_ref, target_ref, normed_ref, out_ref):
    rows = out_ref.shape[0]
    tokens = normed_ref.shape[0]
    row = lax.broadcasted_iota(jnp.int32, (rows, tokens), 0)
    place = row % 8
    first = (row // 8) * 16 + chunk_ref[0] * SLOTS

    def picks(slot):
        hit = target_ref[0:1, :] == slot
        for k in range(1, TOPK):
            hit = hit | (target_ref[k : k + 1, :] == slot)
        return jnp.where(hit, 1.0, 0.0).astype(jnp.bfloat16)

    main = picks(jnp.where(place < SLOTS, first + place, -1))
    last = normed_ref[:, BLOCKS * LANES :]
    for b in range(BLOCKS):
        extra = picks(jnp.where(place < SLOTS, -1, first + 2 * b + place - SLOTS))
        cols = slice(b * LANES, (b + 1) * LANES)
        out_ref[:, cols] = (dot(main, normed_ref[:, cols]) + dot(extra, last)).astype(out_ref.dtype)


def dispatched(chunk, target, normed, rows):
    vmem = pl.BlockSpec(memory_space=pltpu.VMEM)
    return pl.pallas_call(
        dispatch_kernel,
        in_specs=[pl.BlockSpec(memory_space=pltpu.SMEM), vmem, vmem],
        out_specs=vmem,
        out_shape=jax.ShapeDtypeStruct((rows, BLOCKS * LANES), jnp.bfloat16),
        compiler_params=params(12),
        cost_estimate=cost(4 * rows * 128 * 768, 1 << 20),
        name="dispatch",
    )(jnp.full((1,), chunk, jnp.int32), target, normed)


def hidden_kernel(tp_ref, own, nt, nb, ft, fb, pt, pb, gate_ref, up_ref, out_ref, held, acc, sems):
    step = pl.program_id(0)
    rows = own.shape[0]
    width = BLOCKS * LANES
    half = rows // 2
    copies = [pltpu.make_async_copy(own, held.at[0], sems.at[0])]
    for j, (top, bottom) in enumerate(((nt, nb), (ft, fb), (pt, pb))):
        for k, piece in enumerate((top, bottom)):
            copies.append(
                pltpu.make_async_copy(
                    piece, held.at[j + 1, pl.ds(k * half, half)], sems.at[1 + 2 * j + k]
                )
            )

    @pl.when(step == 0)
    def _():
        for copy in copies:
            copy.start()
        acc[...] = jnp.zeros(acc.shape, acc.dtype)
        copies[0].wait()

    for j in range(1, N_TP):

        @pl.when(step == j)
        def _():
            copies[2 * j - 1].wait()
            copies[2 * j].wait()

    shape = (rows // 8, 8, LANES)
    place = lax.broadcasted_iota(jnp.int32, shape, 1)
    moved = [
        pltpu.roll(
            held[step, :, b * LANES : (b + 1) * LANES].astype(jnp.float32).reshape(shape), 2 * b + 2, 1
        )
        for b in range(BLOCKS)
    ]
    last = jnp.where(place < 2, moved[0], jnp.where(place < 4, moved[1], moved[2]))
    last = last.reshape(rows, LANES).astype(jnp.bfloat16)
    for side, w_ref in enumerate((gate_ref, up_ref)):
        acc[side] += dot(held[step], w_ref[:width, :]) + dot(last, w_ref[width:, :])

    @pl.when(step == N_TP - 1)
    def _():
        gate_cut = jnp.minimum(acc[0], CLAMP)
        up_cut = jnp.clip(acc[1], -CLAMP, CLAMP)
        value = ((up_cut + 1.0) * gate_cut * jax.nn.sigmoid(SLOPE * gate_cut)).reshape(shape)
        count = rows // 32
        low = place[:count] < SLOTS
        fourth = value[BLOCKS * count :]
        for b in range(BLOCKS):
            packed = jnp.where(
                low, value[b * count : (b + 1) * count], pltpu.roll(fourth, SLOTS - 2 * b, 1)
            )
            out_ref[b * count * 8 : (b + 1) * count * 8, :] = packed.reshape(count * 8, LANES).astype(
                out_ref.dtype
            )


def hidden(tp, own, pieces, gate, up):
    rows, width = own.shape
    cols = gate.shape[1]
    weight = pl.BlockSpec((width + LANES, cols), lambda j, t: ((t[0] + j) % N_TP, 0))
    return pl.pallas_call(
        hidden_kernel,
        grid_spec=pltpu.PrefetchScalarGridSpec(
            num_scalar_prefetch=1,
            grid=(N_TP,),
            in_specs=[pl.BlockSpec(memory_space=pl.ANY)] * 7 + [weight] * 2,
            out_specs=pl.BlockSpec((rows * 3 // 4, cols), lambda j, t: (0, 0)),
            scratch_shapes=[
                pltpu.VMEM((N_TP, rows, width), jnp.bfloat16),
                pltpu.VMEM((2, rows, cols), jnp.float32),
                pltpu.SemaphoreType.DMA((7,)),
            ],
        ),
        out_shape=jax.ShapeDtypeStruct((rows * 3 // 4, cols), jnp.bfloat16),
        compiler_params=params(56),
        cost_estimate=cost(8 * rows * width * cols, 8 << 20),
        name="hidden",
    )(tp, own, *pieces, gate, up)


def result_kernel(a0, a1, a2, a3, d0, d1, d2, d3, out_ref):
    res = dot(a0[...], d0[...])
    for a, d in ((a1, d1), (a2, d2), (a3, d3)):
        res = res + dot(a[...], d[...])
    count = res.shape[0] // 24
    shape = (BLOCKS * count, 8, LANES)
    place = lax.broadcasted_iota(jnp.int32, (count, 8, LANES), 1)

    def unpacked(cols):
        value = res[:, cols].reshape(shape)
        parts = [value[b * count : (b + 1) * count] for b in range(BLOCKS)]
        moved = [pltpu.roll(part, 2 * b + 2, 1) for b, part in enumerate(parts)]
        return parts + [jnp.where(place < 2, moved[0], jnp.where(place < 4, moved[1], moved[2]))]

    last = unpacked(slice(BLOCKS * LANES, (BLOCKS + 1) * LANES))
    for b in range(BLOCKS):
        main = unpacked(slice(b * LANES, (b + 1) * LANES))
        for q in range(4):
            block = jnp.where(place < SLOTS, main[q], pltpu.roll(last[q], SLOTS - 2 * b, 1))
            out_ref[q * count * 8 : (q + 1) * count * 8, b * LANES : (b + 1) * LANES] = block.reshape(
                count * 8, LANES
            ).astype(out_ref.dtype)


def results(acts, downs):
    rows = acts[0].shape[0]
    return pl.pallas_call(
        result_kernel,
        out_shape=jax.ShapeDtypeStruct((rows * 4 // 3, BLOCKS * LANES), jnp.bfloat16),
        compiler_params=params(14),
        cost_estimate=cost(2 * rows * 1024 * 1024, 4 << 20),
        name="results",
    )(*acts, *downs)


def combine_kernel(chunk_ref, target_ref, weight_ref, back_ref, before_ref, sum_ref, out_ref):
    tokens = target_ref.shape[0]
    rows = back_ref.shape[0]
    lane = lax.broadcasted_iota(jnp.int32, (tokens, rows), 1)
    place = lane % 8
    first = (lane // 8) * 16 + chunk_ref[0] * SLOTS

    def mixing(slot):
        mix = jnp.zeros((tokens, rows), jnp.float32)
        for k in range(TOPK):
            mix = jnp.where(target_ref[:, k : k + 1] == slot, weight_ref[:, k : k + 1], mix)
        main = mix.astype(jnp.bfloat16)
        return main, (mix - main.astype(jnp.float32)).astype(jnp.bfloat16)

    main = mixing(jnp.where(place < SLOTS, first + place, -1))
    last = jnp.zeros((tokens, LANES), jnp.float32)
    for b in range(BLOCKS + 1):
        cols = slice(b * LANES, (b + 1) * LANES)
        if b < BLOCKS:
            block = back_ref[:, cols]
            extra = mixing(jnp.where(place < SLOTS, -1, first + 2 * b + place - SLOTS))
            last = last + dot(extra[0], block) + dot(extra[1], block)
            value = dot(main[0], block) + dot(main[1], block)
        else:
            value = last
        value = value + before_ref[:, cols]
        sum_ref[:, cols] = value
        out_ref[:, cols] = value.astype(out_ref.dtype)


def combined(chunk, target, weight, back, before):
    vmem = pl.BlockSpec(memory_space=pltpu.VMEM)
    return pl.pallas_call(
        combine_kernel,
        in_specs=[pl.BlockSpec(memory_space=pltpu.SMEM)] + [vmem] * 4,
        out_specs=[vmem] * 2,
        out_shape=[
            jax.ShapeDtypeStruct(before.shape, jnp.float32),
            jax.ShapeDtypeStruct(before.shape, jnp.bfloat16),
        ],
        compiler_params=params(12),
        cost_estimate=cost(10**9, 2 << 20),
        name="combine",
    )(jnp.full((1,), chunk, jnp.int32), target, weight, back, before)


def program(
    projected_queries,
    key_proj,
    projected_values,
    head_sink_logits,
    out_weight,
    expert_input,
    norm_gain,
    routing,
    route_weight,
    gate_weight,
    up_weight,
    down_weight,
):
    bf = jnp.bfloat16
    tp = lax.axis_index("tp")
    at = tp.astype(jnp.int32).reshape(1)
    token_rows = expert_input.shape[0]
    experts = lax.axis_size("ep")
    share = D // N_TP

    ids = routing.T.reshape(-1)
    index = jnp.arange(ids.shape[0])
    same = (ids[:, None] == ids[None, :]) & (index[:, None] < index[None, :])
    rank = jnp.sum(same.astype(jnp.int32), axis=0)
    target = (ids * 16 + rank).reshape(TOPK, token_rows)

    widened = expert_input.astype(jnp.float32)
    scale = lax.rsqrt(jnp.mean(widened * widened, axis=-1, keepdims=True) + EPS)
    own = lax.dynamic_slice_in_dim(expert_input, tp * share, share, 1).astype(jnp.float32)
    gain = lax.dynamic_slice_in_dim(norm_gain, tp * share, share, 0)
    normed = (own * scale * gain[None, :]).astype(bf)

    got1 = exchanged(dispatched(0, target, normed, experts * 8))
    got2 = exchanged(dispatched(1, target, normed, experts * 8))

    downs = []
    for k in range(N_TP):
        block = lax.dynamic_slice_in_dim(down_weight[0], ((tp + N_TP - k) % N_TP) * share, share, 1)
        downs.append(shifted(block, k) if k else block)

    def activated(got):
        middle = got.shape[0] // 2
        top, bottom = got[:middle], got[middle:]
        nt, pt = shifted(top, 1), shifted(top, -1)
        nb, pb = shifted(bottom, 1), shifted(bottom, -1)
        ft, fb = shifted(nt, 1), shifted(pb, -1)
        return hidden(at, got, (nt, nb, ft, fb, pt, pb), gate_weight[0], up_weight[0])

    def spread(act):
        return (act, shifted(act, 1), shifted(act, 2), shifted(act, -1))

    back1 = exchanged(results(spread(activated(got1)), downs))
    back2 = exchanged(results(spread(activated(got2)), downs))

    attended = attention(projected_queries, key_proj, projected_values, head_sink_logits)
    partial = dot(attended, out_weight).astype(bf)
    owned = partial.shape[0] // N_TP
    mixed = None
    for k in range(N_TP):
        block = lax.dynamic_slice_in_dim(partial, ((tp + N_TP - k) % N_TP) * owned, owned, 0)
        block = (shifted(block, k) if k else block).astype(jnp.float32)
        mixed = block if mixed is None else mixed + block
    mixer_output = mixed.astype(bf)

    columns = target.T
    start = jnp.zeros((token_rows, share), jnp.float32)
    so_far = combined(0, columns, route_weight, back1, start)[0]
    expert_output = combined(1, columns, route_weight, back2, so_far)[1]
    return (mixer_output, expert_output)


def solution(mesh):
    placed = (
        P("ep", "tp"),
        P("ep", "tp"),
        P("ep", "tp"),
        P("tp"),
        P("tp", None),
        P("ep", None),
        P(),
        P("ep", None),
        P("ep", None),
        P("ep", None, "tp"),
        P("ep", None, "tp"),
        P("ep", "tp", None),
    )
    return jax.shard_map(
        program,
        mesh=mesh,
        in_specs=placed,
        out_specs=(P(("ep", "tp"), None), P("ep", "tp")),
        check_vma=False,
    )
```

profile of v0, /device:TPU:2, one launch (start us, length us, event | category | flops | bytes accessed | tf_op | source)
XLA Modules:
  0.0 231.7 jit_solution(14200012231306832599)
XLA Ops:
  6.8 12.0 %all-to-all-start.2 = ((bf16[64,8,768]{2,1,0:T(8,128)(2,1)}), bf16[64,8,768]{2,1,0:T(8,128)(2,1)S(1)}, u32[]{:S(2)}, u32[]{:S(2)}) async-start(bf16[64,8,768]{2,1,0:T(8,128)(2,1)} %bitcast.23), calls=%async_computation.2 | async-start | bytes 1572864 | tf_op jit(solution)/shard_map/all_to_all | solution.py:26
  19.0 2.8 %dynamic-slice_bitcast_fusion = (bf16[256,1024]{1,0:T(8,128)(2,1)S(1)}, bf16[256,1024]{1,0:T(8,128)(2,1)}, bf16[256,1024]{1,0:T(8,128)(2,1)S(1)}, bf16[256,1024]{1,0:T(8,128)(2,1)}) fusion(bf16[1,256,4096]{2,1,0:T(8,128)(2,1)} %param.23, s32[]{:T(128)S(6)} %select_n.72, s32[]{:T(128)S(6)} %select_n.70, s32[]{:T(128)S(6)} %select_n.69, s32[]{:T(128)S(6)} %select_n.71), kind=kLoop, calls=%fused_computation.13 | loop fusion | bytes 4194320 | tf_op jit(solution)/shard_map/dynamic_slice | solution.py:332
  21.7 3.0 %collective-permute-start.13 = (bf16[256,1024]{1,0:T(8,128)(2,1)}, bf16[256,1024]{1,0:T(8,128)(2,1)S(1)}, u32[]{:S(2)}, u32[]{:S(2)}) collective-permute-start(bf16[256,1024]{1,0:T(8,128)(2,1)} %get-tuple-element.7), channel_id=1, source_target_pairs={{1,0},{2,1},{3,2},{0,3},{5,4},{6,5},{7,6},{4,7},{9,8},{10,9},{11,1... | collective-permute-start | bytes 1572872 | tf_op jit(solution)/shard_map/ppermute | solution.py:22
  29.1 12.9 %all-to-all-done.2 = bf16[64,8,768]{2,1,0:T(8,128)(2,1)S(1)} async-done(((bf16[64,8,768]{2,1,0:T(8,128)(2,1)}), bf16[64,8,768]{2,1,0:T(8,128)(2,1)S(1)}, u32[]{:S(2)}, u32[]{:S(2)}) %all-to-all-start.2) | async-done | bytes 786464 | tf_op jit(solution)/shard_map/all_to_all | solution.py:26
  42.0 6.1 %all-to-all-start = ((bf16[64,8,768]{2,1,0:T(8,128)(2,1)}), bf16[64,8,768]{2,1,0:T(8,128)(2,1)}, u32[]{:S(2)}, u32[]{:S(2)}) async-start(bf16[64,8,768]{2,1,0:T(8,128)(2,1)} %bitcast.11), calls=%async_computation | async-start | bytes 1572864 | tf_op jit(solution)/shard_map/all_to_all | solution.py:26
  59.2 13.7 %collective-permute-done.16.nt = bf16[256,768]{1,0:T(8,128)(2,1)S(1)} collective-permute-done((bf16[256,768]{1,0:T(8,128)(2,1)}, bf16[256,768]{1,0:T(8,128)(2,1)S(1)}, u32[]{:S(2)}, u32[]{:S(2)}) %collective-permute-start.16) | collective-permute-done | bytes 393248 | tf_op jit(solution)/shard_map/ppermute | solution.py:22
  73.7 2.9 %collective-permute-start.14 = (bf16[256,1024]{1,0:T(8,128)(2,1)}, bf16[256,1024]{1,0:T(8,128)(2,1)S(1)}, u32[]{:S(2)}, u32[]{:S(2)}) collective-permute-start(bf16[256,1024]{1,0:T(8,128)(2,1)} %get-tuple-element.9), channel_id=1, source_target_pairs={{2,0},{3,1},{0,2},{1,3},{6,4},{7,5},{4,6},{5,7},{10,8},{11,9},{8,1... | collective-permute-start | bytes 1572872 | tf_op jit(solution)/shard_map/ppermute | solution.py:22
  77.5 2.3 %collective-permute-start.18 = (bf16[256,768]{1,0:T(8,128)(2,1)}, bf16[256,768]{1,0:T(8,128)(2,1)S(1)}, u32[]{:S(2)}, u32[]{:S(2)}) collective-permute-start(bf16[256,768]{1,0:T(8,128)(2,1)} %copy-done.8), channel_id=1, source_target_pairs={{1,0},{2,1},{3,2},{0,3},{5,4},{6,5},{7,6},{4,7},{9,8},{10,9},{11,1... | collective-permute-start | bytes 1179656 | tf_op jit(solution)/shard_map/ppermute | solution.py:22
  82.0 15.0 %collective-permute-done.18.ft = bf16[256,768]{1,0:T(8,128)(2,1)S(1)} collective-permute-done((bf16[256,768]{1,0:T(8,128)(2,1)}, bf16[256,768]{1,0:T(8,128)(2,1)S(1)}, u32[]{:S(2)}, u32[]{:S(2)}) %collective-permute-start.18) | collective-permute-done | bytes 393248 | tf_op jit(solution)/shard_map/ppermute | solution.py:22
  97.0 2.6 %collective-permute-start.4 = (bf16[256,768]{1,0:T(8,128)(2,1)}, bf16[256,768]{1,0:T(8,128)(2,1)}, u32[]{:S(2)}, u32[]{:S(2)}) collective-permute-start(bf16[256,768]{1,0:T(8,128)(2,1)} %get-tuple-element.16), channel_id=1, source_target_pairs={{1,0},{2,1},{3,2},{0,3},{5,4},{6,5},{7,6},{4,7},{9,8},{10,9},{11,1... | collective-permute-start | bytes 1179656 | tf_op jit(solution)/shard_map/ppermute | solution.py:22
  99.6 8.5 %collective-permute-done.20.fb = bf16[256,768]{1,0:T(8,128)(2,1)} collective-permute-done((bf16[256,768]{1,0:T(8,128)(2,1)}, bf16[256,768]{1,0:T(8,128)(2,1)}, u32[]{:S(2)}, u32[]{:S(2)}) %collective-permute-start.20) | collective-permute-done | bytes 393248 | tf_op jit(solution)/shard_map/ppermute | solution.py:22
  109.5 7.0 %hidden.3.a0 = bf16[384,256]{1,0:T(8,128)(2,1)} custom-call(s32[1]{0:T(128)} %bitcast.10.tp_ref, bf16[512,768]{1,0:T(8,128)(2,1)} %bitcast.64, bf16[256,768]{1,0:T(8,128)(2,1)} %copy-done.8, bf16[256,768]{1,0:T(8,128)(2,1)} %collective-permute-done.17.nb, bf16[256,768]{1,0:T(8,128)(2,1)} %copy-done.11, bf16[256,768]{1,0:T(8,128)(2,1)} %collective-permute-done.20.fb, ...), custom_call_target="tpu_custom_call" | custom-call | flops 805306368 | bytes 8388608 | tf_op jit(solution)/shard_map/hidden/pallas_call | solution.py:193
  119.9 7.1 %collective-permute-done.22.a1 = bf16[384,256]{1,0:T(8,128)(2,1)S(1)} collective-permute-done((bf16[384,256]{1,0:T(8,128)(2,1)}, bf16[384,256]{1,0:T(8,128)(2,1)S(1)}, u32[]{:S(2)}, u32[]{:S(2)}) %collective-permute-start.22) | collective-permute-done | bytes 196640 | tf_op jit(solution)/shard_map/ppermute | solution.py:22
  127.9 2.5 %collective-permute-done.24.a3 = bf16[384,256]{1,0:T(8,128)(2,1)S(1)} collective-permute-done((bf16[384,256]{1,0:T(8,128)(2,1)}, bf16[384,256]{1,0:T(8,128)(2,1)S(1)}, u32[]{:S(2)}, u32[]{:S(2)}) %collective-permute-start.24) | collective-permute-done | bytes 196640 | tf_op jit(solution)/shard_map/ppermute | solution.py:22
  132.3 10.3 %all-to-all-start.3 = ((bf16[64,8,768]{2,1,0:T(8,128)(2,1)}), bf16[64,8,768]{2,1,0:T(8,128)(2,1)S(1)}, u32[]{:S(2)}, u32[]{:S(2)}) async-start(bf16[64,8,768]{2,1,0:T(8,128)(2,1)} %bitcast.27), calls=%async_computation.3 | async-start | bytes 1572864 | tf_op jit(solution)/shard_map/all_to_all | solution.py:26
  146.9 2.1 fusion.1
  150.6 4.4 %collective-permute-done.5.nb = bf16[256,768]{1,0:T(8,128)(2,1)S(1)} collective-permute-done((bf16[256,768]{1,0:T(8,128)(2,1)}, bf16[256,768]{1,0:T(8,128)(2,1)S(1)}, u32[]{:S(2)}, u32[]{:S(2)}) %collective-permute-start.5) | collective-permute-done | bytes 393248 | tf_op jit(solution)/shard_map/ppermute | solution.py:22
  157.0 5.5 %collective-permute-done.6.ft = bf16[256,768]{1,0:T(8,128)(2,1)S(1)} collective-permute-done((bf16[256,768]{1,0:T(8,128)(2,1)}, bf16[256,768]{1,0:T(8,128)(2,1)S(1)}, u32[]{:S(2)}, u32[]{:S(2)}) %collective-permute-start.6) | collective-permute-done | bytes 393248 | tf_op jit(solution)/shard_map/ppermute | solution.py:22
  165.1 6.8 %hidden.2.a0 = bf16[384,256]{1,0:T(8,128)(2,1)} custom-call(s32[1]{0:T(128)} %bitcast.10.tp_ref, bf16[512,768]{1,0:T(8,128)(2,1)} %bitcast.12.own, bf16[256,768]{1,0:T(8,128)(2,1)} %collective-permute-done.4.nt, bf16[256,768]{1,0:T(8,128)(2,1)} %copy-done.9, bf16[256,768]{1,0:T(8,128)(2,1)} %copy-done.12, bf16[256,768]{1,0:T(8,128)(2,1)} %copy-done.13, ...), custom_call_target="tpu_custom_call" | custom-call | flops 805306368 | bytes 8388608 | tf_op jit(solution)/shard_map/hidden/pallas_call | solution.py:193
  175.2 3.2 %collective-permute-start.1 = (bf16[64,4096]{1,0:T(8,128)(2,1)}, bf16[64,4096]{1,0:T(8,128)(2,1)}, u32[]{:S(2)}, u32[]{:S(2)}) collective-permute-start(bf16[64,4096]{1,0:T(8,128)(2,1)} %get-tuple-element.10), channel_id=1, source_target_pairs={{1,0},{2,1},{3,2},{0,3},{5,4},{6,5},{7,6},{4,7},{9,8},{10,9},{11,1... | collective-permute-start | bytes 1572872 | tf_op jit(solution)/shard_map/ppermute | solution.py:22
  181.9 12.6 %collective-permute-done.12.a3 = bf16[384,256]{1,0:T(8,128)(2,1)S(1)} collective-permute-done((bf16[384,256]{1,0:T(8,128)(2,1)}, bf16[384,256]{1,0:T(8,128)(2,1)S(1)}, u32[]{:S(2)}, u32[]{:S(2)}) %collective-permute-start.12) | collective-permute-done | bytes 196640 | tf_op jit(solution)/shard_map/ppermute | solution.py:22
  196.5 10.3 %all-to-all-start.1 = ((bf16[64,8,768]{2,1,0:T(8,128)(2,1)}), bf16[64,8,768]{2,1,0:T(8,128)(2,1)S(1)}, u32[]{:S(2)}, u32[]{:S(2)}) async-start(bf16[64,8,768]{2,1,0:T(8,128)(2,1)} %bitcast.21), calls=%async_computation.1 | async-start | bytes 1572864 | tf_op jit(solution)/shard_map/all_to_all | solution.py:26
  206.9 2.6 %add_convert_fusion = bf16[64,4096]{1,0:T(8,128)(2,1)} fusion(bf16[64,4096]{1,0:T(8,128)(2,1)} %collective-permute-done.3, bf16[64,4096]{1,0:T(8,128)(2,1)} %collective-permute-done.2, bf16[64,4096]{1,0:T(8,128)(2,1)} %collective-permute-done.1, bf16[256,4096]{1,0:T(8,128)(2,1)} %copy-done.2, s32[]{:T(128)S(6)} %select_n.61), kind=kLoop, calls=%fused_computation.10 | loop fusion | flops 2097152 | bytes 2621444 | tf_op jit(solution)/shard_map/convert_element_type | solution.py:357
  211.2 18.7 %all-to-all-done.1 = bf16[64,8,768]{2,1,0:T(8,128)(2,1)S(1)} async-done(((bf16[64,8,768]{2,1,0:T(8,128)(2,1)}), bf16[64,8,768]{2,1,0:T(8,128)(2,1)S(1)}, u32[]{:S(2)}, u32[]{:S(2)}) %all-to-all-start.1) | async-done | bytes 786464 | tf_op jit(solution)/shard_map/all_to_all | solution.py:26
  (122 shorter events, 55.6 us)
Async XLA Ops:
  6.8 35.2 %all-to-all-start.2 = ((bf16[64,8,768]{2,1,0:T(8,128)(2,1)}), bf16[64,8,768]{2,1,0:T(8,128)(2,1)S(1)}, u32[]{:S(2)}, u32[]{:S(2)}) async-start(bf16[64,8,768]{2,1,0:T(8,128)(2,1)} %bitcast.23), calls=%async_computation.2 | async-start | bytes 1572864 | tf_op jit(solution)/shard_map/all_to_all | solution.py:26
  21.7 94.8 %collective-permute-start.13 = (bf16[256,1024]{1,0:T(8,128)(2,1)}, bf16[256,1024]{1,0:T(8,128)(2,1)S(1)}, u32[]{:S(2)}, u32[]{:S(2)}) collective-permute-start(bf16[256,1024]{1,0:T(8,128)(2,1)} %get-tuple-element.7), channel_id=1, source_target_pairs={{1,0},{2,1},{3,2},{0,3},{5,4},{6,5},{7,6},{4,7},{9,8},{10,9},{11,1... | collective-permute-start | bytes 1572872 | tf_op jit(solution)/shard_map/ppermute | solution.py:22
  25.4 25.5 %collective-permute-start = (bf16[128,256]{1,0:T(8,128)(2,1)}, bf16[128,256]{1,0:T(8,128)(2,1)S(1)}, u32[]{:S(2)}, u32[]{:S(2)}) collective-permute-start(bf16[128,256]{1,0:T(8,128)(2,1)} %pad_maximum_fusion.2), channel_id=1, source_target_pairs={{0,4},{4,8},{8,12},{12,16},{16,20},{20,24},{24,28},{28,32},{32,36}... | collective-permute-start | bytes 196616 | tf_op jit(solution)/shard_map/ppermute | solution.py:39
  42.0 37.9 %all-to-all-start = ((bf16[64,8,768]{2,1,0:T(8,128)(2,1)}), bf16[64,8,768]{2,1,0:T(8,128)(2,1)}, u32[]{:S(2)}, u32[]{:S(2)}) async-start(bf16[64,8,768]{2,1,0:T(8,128)(2,1)} %bitcast.11), calls=%async_computation | async-start | bytes 1572864 | tf_op jit(solution)/shard_map/all_to_all | solution.py:26
  51.9 24.7 %collective-permute-start.19 = (bf16[256,768]{1,0:T(8,128)(2,1)}, bf16[256,768]{1,0:T(8,128)(2,1)}, u32[]{:S(2)}, u32[]{:S(2)}) collective-permute-start(bf16[256,768]{1,0:T(8,128)(2,1)} %get-tuple-element.13), channel_id=1, source_target_pairs={{3,0},{0,1},{1,2},{2,3},{7,4},{4,5},{5,6},{6,7},{11,8},{8,9},{9,10... | collective-permute-start | bytes 1179656 | tf_op jit(solution)/shard_map/ppermute | solution.py:22
  53.4 24.0 %collective-permute-start.17 = (bf16[256,768]{1,0:T(8,128)(2,1)}, bf16[256,768]{1,0:T(8,128)(2,1)}, u32[]{:S(2)}, u32[]{:S(2)}) collective-permute-start(bf16[256,768]{1,0:T(8,128)(2,1)} %get-tuple-element.13), channel_id=1, source_target_pairs={{1,0},{2,1},{3,2},{0,3},{5,4},{6,5},{7,6},{4,7},{9,8},{10,9},{11,1... | collective-permute-start | bytes 1179656 | tf_op jit(solution)/shard_map/ppermute | solution.py:22
  55.1 17.8 %collective-permute-start.16 = (bf16[256,768]{1,0:T(8,128)(2,1)}, bf16[256,768]{1,0:T(8,128)(2,1)S(1)}, u32[]{:S(2)}, u32[]{:S(2)}) collective-permute-start(bf16[256,768]{1,0:T(8,128)(2,1)} %get-tuple-element.14), channel_id=1, source_target_pairs={{1,0},{2,1},{3,2},{0,3},{5,4},{6,5},{7,6},{4,7},{9,8},{10,9},{11,1... | collective-permute-start | bytes 1179656 | tf_op jit(solution)/shard_map/ppermute | solution.py:22
  56.9 22.9 %collective-permute-start.21 = (bf16[256,768]{1,0:T(8,128)(2,1)}, bf16[256,768]{1,0:T(8,128)(2,1)}, u32[]{:S(2)}, u32[]{:S(2)}) collective-permute-start(bf16[256,768]{1,0:T(8,128)(2,1)} %get-tuple-element.14), channel_id=1, source_target_pairs={{3,0},{0,1},{1,2},{2,3},{7,4},{4,5},{5,6},{6,7},{11,8},{8,9},{9,10... | collective-permute-start | bytes 1179656 | tf_op jit(solution)/shard_map/ppermute | solution.py:22
  73.7 44.7 %collective-permute-start.14 = (bf16[256,1024]{1,0:T(8,128)(2,1)}, bf16[256,1024]{1,0:T(8,128)(2,1)S(1)}, u32[]{:S(2)}, u32[]{:S(2)}) collective-permute-start(bf16[256,1024]{1,0:T(8,128)(2,1)} %get-tuple-element.9), channel_id=1, source_target_pairs={{2,0},{3,1},{0,2},{1,3},{6,4},{7,5},{4,6},{5,7},{10,8},{11,9},{8,1... | collective-permute-start | bytes 1572872 | tf_op jit(solution)/shard_map/ppermute | solution.py:22
  76.6 42.7 %collective-permute-start.15 = (bf16[256,1024]{1,0:T(8,128)(2,1)S(1)}, bf16[256,1024]{1,0:T(8,128)(2,1)S(1)}, u32[]{:S(2)}, u32[]{:S(2)}) collective-permute-start(bf16[256,1024]{1,0:T(8,128)(2,1)S(1)} %get-tuple-element.6), channel_id=1, source_target_pairs={{3,0},{0,1},{1,2},{2,3},{7,4},{4,5},{5,6},{6,7},{11,8},{8,9},{9,10... | collective-permute-start | bytes 1572872 | tf_op jit(solution)/shard_map/ppermute | solution.py:22
  77.5 19.5 %collective-permute-start.18 = (bf16[256,768]{1,0:T(8,128)(2,1)}, bf16[256,768]{1,0:T(8,128)(2,1)S(1)}, u32[]{:S(2)}, u32[]{:S(2)}) collective-permute-start(bf16[256,768]{1,0:T(8,128)(2,1)} %copy-done.8), channel_id=1, source_target_pairs={{1,0},{2,1},{3,2},{0,3},{5,4},{6,5},{7,6},{4,7},{9,8},{10,9},{11,1... | collective-permute-start | bytes 1179656 | tf_op jit(solution)/shard_map/ppermute | solution.py:22
  79.8 28.2 %collective-permute-start.20 = (bf16[256,768]{1,0:T(8,128)(2,1)}, bf16[256,768]{1,0:T(8,128)(2,1)}, u32[]{:S(2)}, u32[]{:S(2)}) collective-permute-start(bf16[256,768]{1,0:T(8,128)(2,1)} %collective-permute-done.19.pb), channel_id=1, source_target_pairs={{3,0},{0,1},{1,2},{2,3},{7,4},{4,5},{5,6},{6,7},{11,8},{8,9},{9,10... | collective-permute-start | bytes 1179656 | tf_op jit(solution)/shard_map/ppermute | solution.py:22
  97.0 47.8 %collective-permute-start.4 = (bf16[256,768]{1,0:T(8,128)(2,1)}, bf16[256,768]{1,0:T(8,128)(2,1)}, u32[]{:S(2)}, u32[]{:S(2)}) collective-permute-start(bf16[256,768]{1,0:T(8,128)(2,1)} %get-tuple-element.16), channel_id=1, source_target_pairs={{1,0},{2,1},{3,2},{0,3},{5,4},{6,5},{7,6},{4,7},{9,8},{10,9},{11,1... | collective-permute-start | bytes 1179656 | tf_op jit(solution)/shard_map/ppermute | solution.py:22
  108.1 38.8 %collective-permute-start.7 = (bf16[256,768]{1,0:T(8,128)(2,1)}, bf16[256,768]{1,0:T(8,128)(2,1)}, u32[]{:S(2)}, u32[]{:S(2)}) collective-permute-start(bf16[256,768]{1,0:T(8,128)(2,1)} %get-tuple-element.15), channel_id=1, source_target_pairs={{3,0},{0,1},{1,2},{2,3},{7,4},{4,5},{5,6},{6,7},{11,8},{8,9},{9,10... | collective-permute-start | bytes 1179656 | tf_op jit(solution)/shard_map/ppermute | solution.py:22
  132.3 64.1 %all-to-all-start.3 = ((bf16[64,8,768]{2,1,0:T(8,128)(2,1)}), bf16[64,8,768]{2,1,0:T(8,128)(2,1)S(1)}, u32[]{:S(2)}, u32[]{:S(2)}) async-start(bf16[64,8,768]{2,1,0:T(8,128)(2,1)} %bitcast.27), calls=%async_computation.3 | async-start | bytes 1572864 | tf_op jit(solution)/shard_map/all_to_all | solution.py:26
  142.7 12.3 %collective-permute-start.5 = (bf16[256,768]{1,0:T(8,128)(2,1)}, bf16[256,768]{1,0:T(8,128)(2,1)S(1)}, u32[]{:S(2)}, u32[]{:S(2)}) collective-permute-start(bf16[256,768]{1,0:T(8,128)(2,1)} %get-tuple-element.15), channel_id=1, source_target_pairs={{1,0},{2,1},{3,2},{0,3},{5,4},{6,5},{7,6},{4,7},{9,8},{10,9},{11,1... | collective-permute-start | bytes 1179656 | tf_op jit(solution)/shard_map/ppermute | solution.py:22
  143.6 13.4 %collective-permute-start.9 = (bf16[256,768]{1,0:T(8,128)(2,1)}, bf16[256,768]{1,0:T(8,128)(2,1)S(1)}, u32[]{:S(2)}, u32[]{:S(2)}) collective-permute-start(bf16[256,768]{1,0:T(8,128)(2,1)} %get-tuple-element.16), channel_id=1, source_target_pairs={{3,0},{0,1},{1,2},{2,3},{7,4},{4,5},{5,6},{6,7},{11,8},{8,9},{9,10... | collective-permute-start | bytes 1179656 | tf_op jit(solution)/shard_map/ppermute | solution.py:22
  144.8 17.7 %collective-permute-start.6 = (bf16[256,768]{1,0:T(8,128)(2,1)}, bf16[256,768]{1,0:T(8,128)(2,1)S(1)}, u32[]{:S(2)}, u32[]{:S(2)}) collective-permute-start(bf16[256,768]{1,0:T(8,128)(2,1)} %collective-permute-done.4.nt), channel_id=1, source_target_pairs={{1,0},{2,1},{3,2},{0,3},{5,4},{6,5},{7,6},{4,7},{9,8},{10,9},{11,1... | collective-permute-start | bytes 1179656 | tf_op jit(solution)/shard_map/ppermute | solution.py:22
  146.9 17.5 %collective-permute-start.8 = (bf16[256,768]{1,0:T(8,128)(2,1)}, bf16[256,768]{1,0:T(8,128)(2,1)S(1)}, u32[]{:S(2)}, u32[]{:S(2)}) collective-permute-start(bf16[256,768]{1,0:T(8,128)(2,1)} %collective-permute-done.7.pb), channel_id=1, source_target_pairs={{3,0},{0,1},{1,2},{2,3},{7,4},{4,5},{5,6},{6,7},{11,8},{8,9},{9,10... | collective-permute-start | bytes 1179656 | tf_op jit(solution)/shard_map/ppermute | solution.py:22
  174.1 20.4 %collective-permute-start.12 = (bf16[384,256]{1,0:T(8,128)(2,1)}, bf16[384,256]{1,0:T(8,128)(2,1)S(1)}, u32[]{:S(2)}, u32[]{:S(2)}) collective-permute-start(bf16[384,256]{1,0:T(8,128)(2,1)} %hidden.2.a0), channel_id=1, source_target_pairs={{3,0},{0,1},{1,2},{2,3},{7,4},{4,5},{5,6},{6,7},{11,8},{8,9},{9,10... | collective-permute-start | bytes 589832 | tf_op jit(solution)/shard_map/ppermute | solution.py:22
  175.2 31.7 %collective-permute-start.1 = (bf16[64,4096]{1,0:T(8,128)(2,1)}, bf16[64,4096]{1,0:T(8,128)(2,1)}, u32[]{:S(2)}, u32[]{:S(2)}) collective-permute-start(bf16[64,4096]{1,0:T(8,128)(2,1)} %get-tuple-element.10), channel_id=1, source_target_pairs={{1,0},{2,1},{3,2},{0,3},{5,4},{6,5},{7,6},{4,7},{9,8},{10,9},{11,1... | collective-permute-start | bytes 1572872 | tf_op jit(solution)/shard_map/ppermute | solution.py:22
  178.4 28.5 %collective-permute-start.2 = (bf16[64,4096]{1,0:T(8,128)(2,1)}, bf16[64,4096]{1,0:T(8,128)(2,1)}, u32[]{:S(2)}, u32[]{:S(2)}) collective-permute-start(bf16[64,4096]{1,0:T(8,128)(2,1)} %get-tuple-element.12), channel_id=1, source_target_pairs={{2,0},{3,1},{0,2},{1,3},{6,4},{7,5},{4,6},{5,7},{10,8},{11,9},{8,1... | collective-permute-start | bytes 1572872 | tf_op jit(solution)/shard_map/ppermute | solution.py:22
  180.0 26.9 %collective-permute-start.3 = (bf16[64,4096]{1,0:T(8,128)(2,1)S(1)}, bf16[64,4096]{1,0:T(8,128)(2,1)}, u32[]{:S(2)}, u32[]{:S(2)}) collective-permute-start(bf16[64,4096]{1,0:T(8,128)(2,1)S(1)} %get-tuple-element.11), channel_id=1, source_target_pairs={{3,0},{0,1},{1,2},{2,3},{7,4},{4,5},{5,6},{6,7},{11,8},{8,9},{9,10... | collective-permute-start | bytes 1572872 | tf_op jit(solution)/shard_map/ppermute | solution.py:22
  196.5 33.5 %all-to-all-start.1 = ((bf16[64,8,768]{2,1,0:T(8,128)(2,1)}), bf16[64,8,768]{2,1,0:T(8,128)(2,1)S(1)}, u32[]{:S(2)}, u32[]{:S(2)}) async-start(bf16[64,8,768]{2,1,0:T(8,128)(2,1)} %bitcast.21), calls=%async_computation.1 | async-start | bytes 1572864 | tf_op jit(solution)/shard_map/all_to_all | solution.py:26
  (24 other events, 293.0 us)
where the time goes:
time: 233 us; the launch traced here: 232 us
  waiting for transfers between devices  107 us (46%)
  starting transfers between devices  73.7 us (32%)
  Pallas kernels  24.4 us (10%)
  local copies, waits for them, and re-layouts  12.8 us (5%)
  other arithmetic  7.54 us (3%)
  matrix products  5.25 us (2%)
    ppermute x24, waiting for transfers between devices, shifted(): lax.ppermute(block, 'tp', [((i + distance) % N_TP, i) for i in range(N_TP)])  75.3 us
    all_to_all x4, starting transfers between devices, exchanged(): return lax.all_to_all(block, 'ep', split_axis=0, concat_axis=0, tiled=True)  38.7 us
    ppermute x24, starting transfers between devices, shifted(): lax.ppermute(block, 'tp', [((i + distance) % N_TP, i) for i in range(N_TP)])  33.1 us
    all_to_all x4, waiting for transfers between devices, exchanged(): return lax.all_to_all(block, 'ep', split_axis=0, concat_axis=0, tiled=True)  31.6 us
    pallas_call x2, Pallas kernels, hidden(): pl.pallas_call(hidden_kernel, grid_spec=pltpu.PrefetchScalarGridSpec(num_...  13.8 us
  transfers between devices with their start and end apart: 29, of which 15 were waited for; matrix products, arithmetic and copies ran while one was open for 8% of the time, Pallas kernels for 9%

commit v1 on v0

--- a/solution.py
+++ b/solution.py
@@ -28,62 +28,6 @@
 
 def dot(a, b):
     return jnp.dot(a, b, preferred_element_type=jnp.float32)
-
-
-def attention(projected_queries, key_proj, projected_values, head_sink_logits):
-    query_rows = projected_queries.shape[0]
-    kv_heads = key_proj.shape[1] // HEAD_SIZE
-    heads_per_group = projected_queries.shape[1] // HEAD_SIZE // kv_heads
-    count_of_blocks = query_rows // WINDOW_KEYS
-    kept = key_proj.shape[1]
-    prior = lax.ppermute(
-        jnp.concatenate(
-            [key_proj[query_rows - WINDOW_KEYS :], projected_values[query_rows - WINDOW_KEYS :]],
-            axis=1,
-        ),
-        "ep",
-        [(i, i + 1) for i in range(lax.axis_size("ep") - 1)],
-    )
-    prior_key, prior_value = prior[:, :kept], prior[:, kept:]
-    key_all = jnp.concatenate([prior_key, key_proj], axis=0)
-    value_all = jnp.concatenate([prior_value, projected_values], axis=0)
-    window_keys = jnp.concatenate(
-        [
-            key_all[:-WINDOW_KEYS].reshape(count_of_blocks, WINDOW_KEYS, kv_heads, HEAD_SIZE),
-            key_all[WINDOW_KEYS:].reshape(count_of_blocks, WINDOW_KEYS, kv_heads, HEAD_SIZE),
-        ],
-        axis=1,
-    )
-    window_values = jnp.concatenate(
-        [
-            value_all[:-WINDOW_KEYS].reshape(count_of_blocks, WINDOW_KEYS, kv_heads, HEAD_SIZE),
-            value_all[WINDOW_KEYS:].reshape(count_of_blocks, WINDOW_KEYS, kv_heads, HEAD_SIZE),
-        ],
-        axis=1,
-    )
-    query_blocks = projected_queries.reshape(
-        count_of_blocks, WINDOW_KEYS, kv_heads, heads_per_group, HEAD_SIZE
-    )
-    scores = jnp.einsum(
-        "nqhgd,nshd->nhgqs", query_blocks, window_keys, preferred_element_type=jnp.float32
-    ) * HEAD_SIZE ** (-0.5)
-    offset = lax.axis_index("ep") * query_rows
-    block_ids = jnp.arange(count_of_blocks)[:, None, None] * WINDOW_KEYS + offset
-    query_pos = block_ids + jnp.arange(WINDOW_KEYS)[None, :, None]
-    key_pos = block_ids - WINDOW_KEYS + jnp.arange(2 * WINDOW_KEYS)[None, None, :]
-    permitted_mask = (key_pos <= query_pos) & (query_pos - key_pos < WINDOW_KEYS) & (key_pos >= 0)
-    scores = jnp.where(permitted_mask[:, None, None, :, :], scores, -jnp.inf)
-    sink_col = head_sink_logits.reshape(kv_heads, heads_per_group)[None, :, :, None, None]
-    highest = jnp.maximum(jnp.max(scores, axis=-1, keepdims=True), sink_col)
-    numerator = jnp.exp(scores - highest)
-    denominator = jnp.sum(numerator, axis=-1, keepdims=True) + jnp.exp(sink_col - highest)
-    weights = (numerator / denominator).astype(jnp.bfloat16)
-    attended = jnp.einsum(
-        "nhgqs,nshd->nqhgd", weights, window_values, preferred_element_type=jnp.float32
-    )
-    return attended.astype(jnp.bfloat16).reshape(
-        query_rows, kv_heads * heads_per_group * HEAD_SIZE
-    )
 
 
 def params(mib):
@@ -243,6 +187,65 @@
         cost_estimate=cost(2 * rows * 1024 * 1024, 4 << 20),
         name="results",
     )(*acts, *downs)
+
+
+def attention_kernel(ep_ref, sink_ref, q_ref, k_ref, v_ref, prior_ref, out_ref):
+    block = WINDOW_KEYS
+    tiles = q_ref.shape[1] // 128
+    query = lax.broadcasted_iota(jnp.int32, (block, 2 * block), 0)
+    key = lax.broadcasted_iota(jnp.int32, (block, 2 * block), 1)
+    lane = lax.broadcasted_iota(jnp.int32, (block, 128), 1)
+    for n in range(q_ref.shape[0] // block):
+        own = slice(n * block, (n + 1) * block)
+        before = slice((n - 1) * block, n * block)
+        allowed = (key > query) & (key <= query + block)
+        if n == 0:
+            allowed = allowed & (key >= jnp.where(ep_ref[0] == 0, block, 0))
+            key_prior, value_prior = prior_ref[:, :128], prior_ref[:, 128:]
+        else:
+            key_prior, value_prior = k_ref[before, :], v_ref[before, :]
+        keys = jnp.concatenate([key_prior, k_ref[own, :]], axis=0)
+        values = jnp.concatenate([value_prior, v_ref[own, :]], axis=0)
+        for t in range(tiles):
+            tile = q_ref[own, t * 128 : (t + 1) * 128].astype(jnp.float32)
+            group = t // 2
+            parts = []
+            for e in range(2):
+                head = tile if e == group else pltpu.roll(tile, HEAD_SIZE, 1)
+                head = jnp.where(lane // HEAD_SIZE == group, head, 0.0).astype(jnp.bfloat16)
+                scores = lax.dot_general(
+                    head, keys, (((1,), (1,)), ((), ())), preferred_element_type=jnp.float32
+                ) * HEAD_SIZE ** (-0.5)
+                scores = jnp.where(allowed, scores, -jnp.inf)
+                sink = sink_ref[2 * t + e]
+                highest = jnp.maximum(jnp.max(scores, axis=1, keepdims=True), sink)
+                numerator = jnp.exp(scores - highest)
+                denominator = jnp.sum(numerator, axis=1, keepdims=True) + jnp.exp(sink - highest)
+                weights = (numerator * (1.0 / denominator)).astype(jnp.bfloat16)
+                result = dot(weights, values)
+                parts.append(result if e == group else pltpu.roll(result, HEAD_SIZE, 1))
+            out_ref[own, t * 128 : (t + 1) * 128] = jnp.where(
+                lane < HEAD_SIZE, parts[0], parts[1]
+            ).astype(out_ref.dtype)
+
+
+def attention(queries, keys, values, sinks):
+    rows = queries.shape[0]
+    last = [x[rows - WINDOW_KEYS :] for x in (keys, values)]
+    prior = lax.ppermute(
+        jnp.concatenate(last, axis=1), "ep", [(i, i + 1) for i in range(lax.axis_size("ep") - 1)]
+    )
+    vmem = pl.BlockSpec(memory_space=pltpu.VMEM)
+    smem = pl.BlockSpec(memory_space=pltpu.SMEM)
+    return pl.pallas_call(
+        attention_kernel,
+        in_specs=[smem, smem] + [vmem] * 4,
+        out_specs=vmem,
+        out_shape=jax.ShapeDtypeStruct(queries.shape, jnp.bfloat16),
+        compiler_params=params(12),
+        cost_estimate=cost(10**9, 1 << 20),
+        name="attention",
+    )(lax.axis_index("ep").astype(jnp.int32).reshape(1), sinks, queries, keys, values, prior)
 
 
 def combine_kernel(chunk_ref, target_ref, weight_ref, back_ref, before_ref, sum_ref, out_ref):

time: 233 us -> 237 us (1.017)
  waiting for transfers between devices: 107 us -> 113 us
  local copies, waits for them, and re-layouts: 12.8 us -> 9.48 us
  starting transfers between devices: 73.7 us -> 76.3 us
    all_to_all x4, waiting for transfers between devices: 31.6 us -> 40.2 us  [exchanged(): return lax.all_to_all(block, 'ep', split_axis=0, concat_axis=0, tiled=True)]
    dot_general x2 -> x0, matrix products: 3.92 us -> none  [the longest x1 2.08 us: attention(): jnp.einsum('nhgqs,nshd->nqhgd', weights, window_values, preferred_element...]
    ppermute x24, starting transfers between devices: 33.1 us -> 35.7 us  [shifted(): lax.ppermute(block, 'tp', [((i + distance) % N_TP, i) for i in range(N_TP)])]
    ppermute x24, waiting for transfers between devices: 75.3 us -> 72.7 us  [shifted(): lax.ppermute(block, 'tp', [((i + distance) % N_TP, i) for i in range(N_TP)])]
  transfers between devices with their start and end apart: 29 -> 29, of which waited for: 15 -> 18; matrix products, arithmetic and copies ran while one was open for 8% -> 5% of each run, Pallas kernels for 9% -> 10%
where the time goes in v1:
time: 237 us; the launch traced here: 235 us
  waiting for transfers between devices  113 us (48%)
  starting transfers between devices  76.3 us (32%)
  Pallas kernels  26.6 us (11%)
  local copies, waits for them, and re-layouts  9.48 us (4%)
  other arithmetic  5.39 us (2%)
  matrix products  3.45 us (1%)
    ppermute x24, waiting for transfers between devices, shifted(): lax.ppermute(block, 'tp', [((i + distance) % N_TP, i) for i in range(N_TP)])  72.7 us
    all_to_all x4, waiting for transfers between devices, exchanged(): return lax.all_to_all(block, 'ep', split_axis=0, concat_axis=0, tiled=True)  40.2 us
    all_to_all x4, starting transfers between devices, exchanged(): return lax.all_to_all(block, 'ep', split_axis=0, concat_axis=0, tiled=True)  38.7 us
    ppermute x24, starting transfers between devices, shifted(): lax.ppermute(block, 'tp', [((i + distance) % N_TP, i) for i in range(N_TP)])  35.7 us
    pallas_call x2, Pallas kernels, hidden(): pl.pallas_call(hidden_kernel, grid_spec=pltpu.PrefetchScalarGridSpec(num_...  13.6 us
  transfers between devices with their start and end apart: 29, of which 18 were waited for; matrix products, arithmetic and copies ran while one was open for 5% of the time, Pallas kernels for 10%

profile of v1, /device:TPU:2, one launch (start us, length us, event | category | flops | bytes accessed | tf_op | source)
XLA Modules:
  0.0 235.1 jit_solution(15789681613164321229)
XLA Ops:
  6.8 12.0 %all-to-all-start.2 = ((bf16[64,8,768]{2,1,0:T(8,128)(2,1)}), bf16[64,8,768]{2,1,0:T(8,128)(2,1)S(1)}, u32[]{:S(2)}, u32[]{:S(2)}) async-start(bf16[64,8,768]{2,1,0:T(8,128)(2,1)} %bitcast.18), calls=%async_computation.2 | async-start | bytes 1572864 | tf_op jit(solution)/shard_map/all_to_all | solution.py:26
  20.5 21.5 %all-to-all-done.2 = bf16[64,8,768]{2,1,0:T(8,128)(2,1)S(1)} async-done(((bf16[64,8,768]{2,1,0:T(8,128)(2,1)}), bf16[64,8,768]{2,1,0:T(8,128)(2,1)S(1)}, u32[]{:S(2)}, u32[]{:S(2)}) %all-to-all-start.2) | async-done | bytes 786464 | tf_op jit(solution)/shard_map/all_to_all | solution.py:26
  42.0 5.9 %all-to-all-start = ((bf16[64,8,768]{2,1,0:T(8,128)(2,1)}), bf16[64,8,768]{2,1,0:T(8,128)(2,1)}, u32[]{:S(2)}, u32[]{:S(2)}) async-start(bf16[64,8,768]{2,1,0:T(8,128)(2,1)} %bitcast.6), calls=%async_computation | async-start | bytes 1572864 | tf_op jit(solution)/shard_map/all_to_all | solution.py:26
  48.0 3.1 %collective-permute-start.16 = (bf16[256,768]{1,0:T(8,128)(2,1)S(1)}, bf16[256,768]{1,0:T(8,128)(2,1)S(1)}, u32[]{:S(2)}, u32[]{:S(2)}) collective-permute-start(bf16[256,768]{1,0:T(8,128)(2,1)S(1)} %get-tuple-element.14), channel_id=1, source_target_pairs={{1,0},{2,1},{3,2},{0,3},{5,4},{6,5},{7,6},{4,7},{9,8},{10,9},{11,1... | collective-permute-start | bytes 1179656 | tf_op jit(solution)/shard_map/ppermute | solution.py:22
  51.1 3.2 %collective-permute-start.17 = (bf16[256,768]{1,0:T(8,128)(2,1)S(1)}, bf16[256,768]{1,0:T(8,128)(2,1)}, u32[]{:S(2)}, u32[]{:S(2)}) collective-permute-start(bf16[256,768]{1,0:T(8,128)(2,1)S(1)} %get-tuple-element.13), channel_id=1, source_target_pairs={{1,0},{2,1},{3,2},{0,3},{5,4},{6,5},{7,6},{4,7},{9,8},{10,9},{11,1... | collective-permute-start | bytes 1179656 | tf_op jit(solution)/shard_map/ppermute | solution.py:22
  56.1 3.3 %collective-permute-start.13 = (bf16[256,1024]{1,0:T(8,128)(2,1)S(1)}, bf16[256,1024]{1,0:T(8,128)(2,1)S(1)}, u32[]{:S(2)}, u32[]{:S(2)}) collective-permute-start(bf16[256,1024]{1,0:T(8,128)(2,1)S(1)} %get-tuple-element.7), channel_id=1, source_target_pairs={{1,0},{2,1},{3,2},{0,3},{5,4},{6,5},{7,6},{4,7},{9,8},{10,9},{11,1... | collective-permute-start | bytes 1572872 | tf_op jit(solution)/shard_map/ppermute | solution.py:22
  60.6 3.7 %collective-permute-start.18 = (bf16[256,768]{1,0:T(8,128)(2,1)S(1)}, bf16[256,768]{1,0:T(8,128)(2,1)S(1)}, u32[]{:S(2)}, u32[]{:S(2)}) collective-permute-start(bf16[256,768]{1,0:T(8,128)(2,1)S(1)} %collective-permute-done.16.nt), channel_id=1, source_target_pairs={{1,0},{2,1},{3,2},{0,3},{5,4},{6,5},{7,6},{4,7},{9,8},{10,9},{11,1... | collective-permute-start | bytes 1179656 | tf_op jit(solution)/shard_map/ppermute | solution.py:22
  64.4 4.6 %collective-permute-done.17.nb = bf16[256,768]{1,0:T(8,128)(2,1)} collective-permute-done((bf16[256,768]{1,0:T(8,128)(2,1)S(1)}, bf16[256,768]{1,0:T(8,128)(2,1)}, u32[]{:S(2)}, u32[]{:S(2)}) %collective-permute-start.17) | collective-permute-done | bytes 393248 | tf_op jit(solution)/shard_map/ppermute | solution.py:22
  69.0 2.8 %collective-permute-start.14 = (bf16[256,1024]{1,0:T(8,128)(2,1)S(1)}, bf16[256,1024]{1,0:T(8,128)(2,1)S(1)}, u32[]{:S(2)}, u32[]{:S(2)}) collective-permute-start(bf16[256,1024]{1,0:T(8,128)(2,1)S(1)} %get-tuple-element.9), channel_id=1, source_target_pairs={{2,0},{3,1},{0,2},{1,3},{6,4},{7,5},{4,6},{5,7},{10,8},{11,9},{8,1... | collective-permute-start | bytes 1572872 | tf_op jit(solution)/shard_map/ppermute | solution.py:22
  73.7 25.4 %collective-permute-done.18.ft = bf16[256,768]{1,0:T(8,128)(2,1)S(1)} collective-permute-done((bf16[256,768]{1,0:T(8,128)(2,1)S(1)}, bf16[256,768]{1,0:T(8,128)(2,1)S(1)}, u32[]{:S(2)}, u32[]{:S(2)}) %collective-permute-start.18) | collective-permute-done | bytes 393248 | tf_op jit(solution)/shard_map/ppermute | solution.py:22
  100.0 6.8 %hidden.3.a0 = bf16[384,256]{1,0:T(8,128)(2,1)} custom-call(s32[1]{0:T(128)} %bitcast.5.tp_ref, bf16[512,768]{1,0:T(8,128)(2,1)} %bitcast.43, bf16[256,768]{1,0:T(8,128)(2,1)} %copy-done.8, bf16[256,768]{1,0:T(8,128)(2,1)} %collective-permute-done.17.nb, bf16[256,768]{1,0:T(8,128)(2,1)} %copy-done.12, bf16[256,768]{1,0:T(8,128)(2,1)} %copy-done.14, ...), custom_call_target="tpu_custom_call" | custom-call | flops 805306368 | bytes 8388608 | tf_op jit(solution)/shard_map/hidden/pallas_call | solution.py:137
  106.8 3.9 %collective-permute-start.22 = (bf16[384,256]{1,0:T(8,128)(2,1)}, bf16[384,256]{1,0:T(8,128)(2,1)S(1)}, u32[]{:S(2)}, u32[]{:S(2)}) collective-permute-start(bf16[384,256]{1,0:T(8,128)(2,1)} %hidden.3.a0), channel_id=1, source_target_pairs={{1,0},{2,1},{3,2},{0,3},{5,4},{6,5},{7,6},{4,7},{9,8},{10,9},{11,1... | collective-permute-start | bytes 589832 | tf_op jit(solution)/shard_map/ppermute | solution.py:22
  111.7 7.1 %collective-permute-done.22.a1 = bf16[384,256]{1,0:T(8,128)(2,1)S(1)} collective-permute-done((bf16[384,256]{1,0:T(8,128)(2,1)}, bf16[384,256]{1,0:T(8,128)(2,1)S(1)}, u32[]{:S(2)}, u32[]{:S(2)}) %collective-permute-start.22) | collective-permute-done | bytes 196640 | tf_op jit(solution)/shard_map/ppermute | solution.py:22
  125.1 10.5 %all-to-all-start.3 = ((bf16[64,8,768]{2,1,0:T(8,128)(2,1)}), bf16[64,8,768]{2,1,0:T(8,128)(2,1)S(1)}, u32[]{:S(2)}, u32[]{:S(2)}) async-start(bf16[64,8,768]{2,1,0:T(8,128)(2,1)} %bitcast.22), calls=%async_computation.3 | async-start | bytes 1572864 | tf_op jit(solution)/shard_map/all_to_all | solution.py:26
  143.8 6.1 %collective-permute-done.4.nt = bf16[256,768]{1,0:T(8,128)(2,1)} collective-permute-done((bf16[256,768]{1,0:T(8,128)(2,1)}, bf16[256,768]{1,0:T(8,128)(2,1)}, u32[]{:S(2)}, u32[]{:S(2)}) %collective-permute-start.4) | collective-permute-done | bytes 393248 | tf_op jit(solution)/shard_map/ppermute | solution.py:22
  152.1 2.4 %attention.1 = bf16[256,512]{1,0:T(8,128)(2,1)S(1)} custom-call(s32[1]{0:T(128)} %bitcast.ep_ref, f32[8]{0:T(128)S(1)} %copy-done.5, bf16[256,512]{1,0:T(8,128)(2,1)S(1)} %copy-done.4, bf16[256,128]{1,0:T(8,128)(2,1)S(1)} %copy-done.2, bf16[256,128]{1,0:T(8,128)(2,1)S(1)} %copy-done.3, bf16[128,256]{1,0:T(8,128)(2,1)S(1)} %collective-permute-done.prior_ref), custom_call_target="tpu_custom_call" | custom-call | flops 1000000000 | bytes 1048576 | tf_op jit(solution)/shard_map/attention/pallas_call | solution.py:240
  154.4 3.4 %convolution_convert_fusion = bf16[256,4096]{1,0:T(8,128)(2,1)S(1)} fusion(bf16[256,512]{1,0:T(8,128)(2,1)S(1)} %attention.1, bf16[512,4096]{1,0:T(8,128)(2,1)} %param.16), kind=kOutput, calls=%fused_computation | convolution fusion | flops 1074790400 | bytes 6553600 | tf_op jit(solution)/shard_map/dot_general | solution.py:30
  160.3 5.5 %collective-permute-done.6.ft = bf16[256,768]{1,0:T(8,128)(2,1)S(1)} collective-permute-done((bf16[256,768]{1,0:T(8,128)(2,1)}, bf16[256,768]{1,0:T(8,128)(2,1)S(1)}, u32[]{:S(2)}, u32[]{:S(2)}) %collective-permute-start.6) | collective-permute-done | bytes 393248 | tf_op jit(solution)/shard_map/ppermute | solution.py:22
  168.4 6.8 %hidden.2.a0 = bf16[384,256]{1,0:T(8,128)(2,1)} custom-call(s32[1]{0:T(128)} %bitcast.5.tp_ref, bf16[512,768]{1,0:T(8,128)(2,1)} %bitcast.7.own, bf16[256,768]{1,0:T(8,128)(2,1)} %collective-permute-done.4.nt, bf16[256,768]{1,0:T(8,128)(2,1)} %copy-done.9, bf16[256,768]{1,0:T(8,128)(2,1)} %copy-done.11, bf16[256,768]{1,0:T(8,128)(2,1)} %copy-done.13, ...), custom_call_target="tpu_custom_call" | custom-call | flops 805306368 | bytes 8388608 | tf_op jit(solution)/shard_map/hidden/pallas_call | solution.py:137
  178.7 3.2 %collective-permute-start.1 = (bf16[64,4096]{1,0:T(8,128)(2,1)}, bf16[64,4096]{1,0:T(8,128)(2,1)}, u32[]{:S(2)}, u32[]{:S(2)}) collective-permute-start(bf16[64,4096]{1,0:T(8,128)(2,1)} %get-tuple-element.10), channel_id=1, source_target_pairs={{1,0},{2,1},{3,2},{0,3},{5,4},{6,5},{7,6},{4,7},{9,8},{10,9},{11,1... | collective-permute-start | bytes 1572872 | tf_op jit(solution)/shard_map/ppermute | solution.py:22
  185.4 12.5 %collective-permute-done.12.a3 = bf16[384,256]{1,0:T(8,128)(2,1)S(1)} collective-permute-done((bf16[384,256]{1,0:T(8,128)(2,1)}, bf16[384,256]{1,0:T(8,128)(2,1)S(1)}, u32[]{:S(2)}, u32[]{:S(2)}) %collective-permute-start.12) | collective-permute-done | bytes 196640 | tf_op jit(solution)/shard_map/ppermute | solution.py:22
  199.9 10.3 %all-to-all-start.1 = ((bf16[64,8,768]{2,1,0:T(8,128)(2,1)}), bf16[64,8,768]{2,1,0:T(8,128)(2,1)S(1)}, u32[]{:S(2)}, u32[]{:S(2)}) async-start(bf16[64,8,768]{2,1,0:T(8,128)(2,1)} %bitcast.16), calls=%async_computation.1 | async-start | bytes 1572864 | tf_op jit(solution)/shard_map/all_to_all | solution.py:26
  210.4 2.6 %add_convert_fusion = bf16[64,4096]{1,0:T(8,128)(2,1)} fusion(bf16[64,4096]{1,0:T(8,128)(2,1)} %collective-permute-done.3, bf16[64,4096]{1,0:T(8,128)(2,1)} %collective-permute-done.2, bf16[64,4096]{1,0:T(8,128)(2,1)} %collective-permute-done.1, bf16[256,4096]{1,0:T(8,128)(2,1)} %copy-done.7, s32[]{:T(128)S(6)} %select_n.56), kind=kLoop, calls=%fused_computation.4 | loop fusion | flops 2097152 | bytes 2621444 | tf_op jit(solution)/shard_map/convert_element_type | solution.py:360
  214.6 18.7 %all-to-all-done.1 = bf16[64,8,768]{2,1,0:T(8,128)(2,1)S(1)} async-done(((bf16[64,8,768]{2,1,0:T(8,128)(2,1)}), bf16[64,8,768]{2,1,0:T(8,128)(2,1)S(1)}, u32[]{:S(2)}, u32[]{:S(2)}) %all-to-all-start.1) | async-done | bytes 786464 | tf_op jit(solution)/shard_map/all_to_all | solution.py:26
  (98 shorter events, 48.8 us)
Async XLA Ops:
  6.8 35.2 %all-to-all-start.2 = ((bf16[64,8,768]{2,1,0:T(8,128)(2,1)}), bf16[64,8,768]{2,1,0:T(8,128)(2,1)S(1)}, u32[]{:S(2)}, u32[]{:S(2)}) async-start(bf16[64,8,768]{2,1,0:T(8,128)(2,1)} %bitcast.18), calls=%async_computation.2 | async-start | bytes 1572864 | tf_op jit(solution)/shard_map/all_to_all | solution.py:26
  42.0 83.1 %all-to-all-start = ((bf16[64,8,768]{2,1,0:T(8,128)(2,1)}), bf16[64,8,768]{2,1,0:T(8,128)(2,1)}, u32[]{:S(2)}, u32[]{:S(2)}) async-start(bf16[64,8,768]{2,1,0:T(8,128)(2,1)} %bitcast.6), calls=%async_computation | async-start | bytes 1572864 | tf_op jit(solution)/shard_map/all_to_all | solution.py:26
  48.0 12.6 %collective-permute-start.16 = (bf16[256,768]{1,0:T(8,128)(2,1)S(1)}, bf16[256,768]{1,0:T(8,128)(2,1)S(1)}, u32[]{:S(2)}, u32[]{:S(2)}) collective-permute-start(bf16[256,768]{1,0:T(8,128)(2,1)S(1)} %get-tuple-element.14), channel_id=1, source_target_pairs={{1,0},{2,1},{3,2},{0,3},{5,4},{6,5},{7,6},{4,7},{9,8},{10,9},{11,1... | collective-permute-start | bytes 1179656 | tf_op jit(solution)/shard_map/ppermute | solution.py:22
  51.1 13.3 %collective-permute-start.19 = (bf16[256,768]{1,0:T(8,128)(2,1)S(1)}, bf16[256,768]{1,0:T(8,128)(2,1)}, u32[]{:S(2)}, u32[]{:S(2)}) collective-permute-start(bf16[256,768]{1,0:T(8,128)(2,1)S(1)} %get-tuple-element.13), channel_id=1, source_target_pairs={{3,0},{0,1},{1,2},{2,3},{7,4},{4,5},{5,6},{6,7},{11,8},{8,9},{9,10... | collective-permute-start | bytes 1179656 | tf_op jit(solution)/shard_map/ppermute | solution.py:22
  51.1 17.9 %collective-permute-start.17 = (bf16[256,768]{1,0:T(8,128)(2,1)S(1)}, bf16[256,768]{1,0:T(8,128)(2,1)}, u32[]{:S(2)}, u32[]{:S(2)}) collective-permute-start(bf16[256,768]{1,0:T(8,128)(2,1)S(1)} %get-tuple-element.13), channel_id=1, source_target_pairs={{1,0},{2,1},{3,2},{0,3},{5,4},{6,5},{7,6},{4,7},{9,8},{10,9},{11,1... | collective-permute-start | bytes 1179656 | tf_op jit(solution)/shard_map/ppermute | solution.py:22
  54.3 18.5 %collective-permute-start.21 = (bf16[256,768]{1,0:T(8,128)(2,1)S(1)}, bf16[256,768]{1,0:T(8,128)(2,1)}, u32[]{:S(2)}, u32[]{:S(2)}) collective-permute-start(bf16[256,768]{1,0:T(8,128)(2,1)S(1)} %get-tuple-element.14), channel_id=1, source_target_pairs={{3,0},{0,1},{1,2},{2,3},{7,4},{4,5},{5,6},{6,7},{11,8},{8,9},{9,10... | collective-permute-start | bytes 1179656 | tf_op jit(solution)/shard_map/ppermute | solution.py:22
  56.1 54.6 %collective-permute-start.13 = (bf16[256,1024]{1,0:T(8,128)(2,1)S(1)}, bf16[256,1024]{1,0:T(8,128)(2,1)S(1)}, u32[]{:S(2)}, u32[]{:S(2)}) collective-permute-start(bf16[256,1024]{1,0:T(8,128)(2,1)S(1)} %get-tuple-element.7), channel_id=1, source_target_pairs={{1,0},{2,1},{3,2},{0,3},{5,4},{6,5},{7,6},{4,7},{9,8},{10,9},{11,1... | collective-permute-start | bytes 1572872 | tf_op jit(solution)/shard_map/ppermute | solution.py:22
  60.6 38.5 %collective-permute-start.18 = (bf16[256,768]{1,0:T(8,128)(2,1)S(1)}, bf16[256,768]{1,0:T(8,128)(2,1)S(1)}, u32[]{:S(2)}, u32[]{:S(2)}) collective-permute-start(bf16[256,768]{1,0:T(8,128)(2,1)S(1)} %collective-permute-done.16.nt), channel_id=1, source_target_pairs={{1,0},{2,1},{3,2},{0,3},{5,4},{6,5},{7,6},{4,7},{9,8},{10,9},{11,1... | collective-permute-start | bytes 1179656 | tf_op jit(solution)/shard_map/ppermute | solution.py:22
  64.4 34.7 %collective-permute-start.20 = (bf16[256,768]{1,0:T(8,128)(2,1)}, bf16[256,768]{1,0:T(8,128)(2,1)S(1)}, u32[]{:S(2)}, u32[]{:S(2)}) collective-permute-start(bf16[256,768]{1,0:T(8,128)(2,1)} %collective-permute-done.19.pb), channel_id=1, source_target_pairs={{3,0},{0,1},{1,2},{2,3},{7,4},{4,5},{5,6},{6,7},{11,8},{8,9},{9,10... | collective-permute-start | bytes 1179656 | tf_op jit(solution)/shard_map/ppermute | solution.py:22
  69.0 42.7 %collective-permute-start.14 = (bf16[256,1024]{1,0:T(8,128)(2,1)S(1)}, bf16[256,1024]{1,0:T(8,128)(2,1)S(1)}, u32[]{:S(2)}, u32[]{:S(2)}) collective-permute-start(bf16[256,1024]{1,0:T(8,128)(2,1)S(1)} %get-tuple-element.9), channel_id=1, source_target_pairs={{2,0},{3,1},{0,2},{1,3},{6,4},{7,5},{4,6},{5,7},{10,8},{11,9},{8,1... | collective-permute-start | bytes 1572872 | tf_op jit(solution)/shard_map/ppermute | solution.py:22
  72.8 38.9 %collective-permute-start.15 = (bf16[256,1024]{1,0:T(8,128)(2,1)S(1)}, bf16[256,1024]{1,0:T(8,128)(2,1)S(1)}, u32[]{:S(2)}, u32[]{:S(2)}) collective-permute-start(bf16[256,1024]{1,0:T(8,128)(2,1)S(1)} %get-tuple-element.6), channel_id=1, source_target_pairs={{3,0},{0,1},{1,2},{2,3},{7,4},{4,5},{5,6},{6,7},{11,8},{8,9},{9,10... | collective-permute-start | bytes 1572872 | tf_op jit(solution)/shard_map/ppermute | solution.py:22
  125.1 74.8 %all-to-all-start.3 = ((bf16[64,8,768]{2,1,0:T(8,128)(2,1)}), bf16[64,8,768]{2,1,0:T(8,128)(2,1)S(1)}, u32[]{:S(2)}, u32[]{:S(2)}) async-start(bf16[64,8,768]{2,1,0:T(8,128)(2,1)} %bitcast.22), calls=%async_computation.3 | async-start | bytes 1572864 | tf_op jit(solution)/shard_map/all_to_all | solution.py:26
  137.6 12.3 %collective-permute-start.4 = (bf16[256,768]{1,0:T(8,128)(2,1)}, bf16[256,768]{1,0:T(8,128)(2,1)}, u32[]{:S(2)}, u32[]{:S(2)}) collective-permute-start(bf16[256,768]{1,0:T(8,128)(2,1)} %get-tuple-element.16), channel_id=1, source_target_pairs={{1,0},{2,1},{3,2},{0,3},{5,4},{6,5},{7,6},{4,7},{9,8},{10,9},{11,1... | collective-permute-start | bytes 1179656 | tf_op jit(solution)/shard_map/ppermute | solution.py:22
  138.5 13.5 %collective-permute-start.7 = (bf16[256,768]{1,0:T(8,128)(2,1)}, bf16[256,768]{1,0:T(8,128)(2,1)}, u32[]{:S(2)}, u32[]{:S(2)}) collective-permute-start(bf16[256,768]{1,0:T(8,128)(2,1)} %get-tuple-element.15), channel_id=1, source_target_pairs={{3,0},{0,1},{1,2},{2,3},{7,4},{4,5},{5,6},{6,7},{11,8},{8,9},{9,10... | collective-permute-start | bytes 1179656 | tf_op jit(solution)/shard_map/ppermute | solution.py:22
  139.6 12.4 %collective-permute-start = (bf16[128,256]{1,0:T(8,128)(2,1)S(1)}, bf16[128,256]{1,0:T(8,128)(2,1)S(1)}, u32[]{:S(2)}, u32[]{:S(2)}) collective-permute-start(bf16[128,256]{1,0:T(8,128)(2,1)S(1)} %pad_maximum_fusion), channel_id=1, source_target_pairs={{0,4},{4,8},{8,12},{12,16},{16,20},{20,24},{24,28},{28,32},{32,36}... | collective-permute-start | bytes 196616 | tf_op jit(solution)/shard_map/ppermute | solution.py:235
  141.6 16.6 %collective-permute-start.5 = (bf16[256,768]{1,0:T(8,128)(2,1)}, bf16[256,768]{1,0:T(8,128)(2,1)S(1)}, u32[]{:S(2)}, u32[]{:S(2)}) collective-permute-start(bf16[256,768]{1,0:T(8,128)(2,1)} %get-tuple-element.15), channel_id=1, source_target_pairs={{1,0},{2,1},{3,2},{0,3},{5,4},{6,5},{7,6},{4,7},{9,8},{10,9},{11,1... | collective-permute-start | bytes 1179656 | tf_op jit(solution)/shard_map/ppermute | solution.py:22
  143.8 16.5 %collective-permute-start.9 = (bf16[256,768]{1,0:T(8,128)(2,1)}, bf16[256,768]{1,0:T(8,128)(2,1)S(1)}, u32[]{:S(2)}, u32[]{:S(2)}) collective-permute-start(bf16[256,768]{1,0:T(8,128)(2,1)} %get-tuple-element.16), channel_id=1, source_target_pairs={{3,0},{0,1},{1,2},{2,3},{7,4},{4,5},{5,6},{6,7},{11,8},{8,9},{9,10... | collective-permute-start | bytes 1179656 | tf_op jit(solution)/shard_map/ppermute | solution.py:22
  149.9 15.9 %collective-permute-start.6 = (bf16[256,768]{1,0:T(8,128)(2,1)}, bf16[256,768]{1,0:T(8,128)(2,1)S(1)}, u32[]{:S(2)}, u32[]{:S(2)}) collective-permute-start(bf16[256,768]{1,0:T(8,128)(2,1)} %collective-permute-done.4.nt), channel_id=1, source_target_pairs={{1,0},{2,1},{3,2},{0,3},{5,4},{6,5},{7,6},{4,7},{9,8},{10,9},{11,1... | collective-permute-start | bytes 1179656 | tf_op jit(solution)/shard_map/ppermute | solution.py:22
  152.0 15.6 %collective-permute-start.8 = (bf16[256,768]{1,0:T(8,128)(2,1)}, bf16[256,768]{1,0:T(8,128)(2,1)S(1)}, u32[]{:S(2)}, u32[]{:S(2)}) collective-permute-start(bf16[256,768]{1,0:T(8,128)(2,1)} %collective-permute-done.7.pb), channel_id=1, source_target_pairs={{3,0},{0,1},{1,2},{2,3},{7,4},{4,5},{5,6},{6,7},{11,8},{8,9},{9,10... | collective-permute-start | bytes 1179656 | tf_op jit(solution)/shard_map/ppermute | solution.py:22
  177.5 20.4 %collective-permute-start.12 = (bf16[384,256]{1,0:T(8,128)(2,1)}, bf16[384,256]{1,0:T(8,128)(2,1)S(1)}, u32[]{:S(2)}, u32[]{:S(2)}) collective-permute-start(bf16[384,256]{1,0:T(8,128)(2,1)} %hidden.2.a0), channel_id=1, source_target_pairs={{3,0},{0,1},{1,2},{2,3},{7,4},{4,5},{5,6},{6,7},{11,8},{8,9},{9,10... | collective-permute-start | bytes 589832 | tf_op jit(solution)/shard_map/ppermute | solution.py:22
  178.7 31.7 %collective-permute-start.1 = (bf16[64,4096]{1,0:T(8,128)(2,1)}, bf16[64,4096]{1,0:T(8,128)(2,1)}, u32[]{:S(2)}, u32[]{:S(2)}) collective-permute-start(bf16[64,4096]{1,0:T(8,128)(2,1)} %get-tuple-element.10), channel_id=1, source_target_pairs={{1,0},{2,1},{3,2},{0,3},{5,4},{6,5},{7,6},{4,7},{9,8},{10,9},{11,1... | collective-permute-start | bytes 1572872 | tf_op jit(solution)/shard_map/ppermute | solution.py:22
  181.9 28.5 %collective-permute-start.2 = (bf16[64,4096]{1,0:T(8,128)(2,1)}, bf16[64,4096]{1,0:T(8,128)(2,1)}, u32[]{:S(2)}, u32[]{:S(2)}) collective-permute-start(bf16[64,4096]{1,0:T(8,128)(2,1)} %get-tuple-element.12), channel_id=1, source_target_pairs={{2,0},{3,1},{0,2},{1,3},{6,4},{7,5},{4,6},{5,7},{10,8},{11,9},{8,1... | collective-permute-start | bytes 1572872 | tf_op jit(solution)/shard_map/ppermute | solution.py:22
  183.5 26.9 %collective-permute-start.3 = (bf16[64,4096]{1,0:T(8,128)(2,1)S(1)}, bf16[64,4096]{1,0:T(8,128)(2,1)}, u32[]{:S(2)}, u32[]{:S(2)}) collective-permute-start(bf16[64,4096]{1,0:T(8,128)(2,1)S(1)} %get-tuple-element.11), channel_id=1, source_target_pairs={{3,0},{0,1},{1,2},{2,3},{7,4},{4,5},{5,6},{6,7},{11,8},{8,9},{9,10... | collective-permute-start | bytes 1572872 | tf_op jit(solution)/shard_map/ppermute | solution.py:22
  199.9 33.5 %all-to-all-start.1 = ((bf16[64,8,768]{2,1,0:T(8,128)(2,1)}), bf16[64,8,768]{2,1,0:T(8,128)(2,1)S(1)}, u32[]{:S(2)}, u32[]{:S(2)}) async-start(bf16[64,8,768]{2,1,0:T(8,128)(2,1)} %bitcast.16), calls=%async_computation.1 | async-start | bytes 1572864 | tf_op jit(solution)/shard_map/all_to_all | solution.py:26
  (23 other events, 331.4 us)

commit v2 on v1

--- a/solution.py
+++ b/solution.py
@@ -38,12 +38,20 @@
     return pl.CostEstimate(flops=flops, bytes_accessed=size, transcendentals=0)
 
 
-def dispatch_kernel(chunk_ref, target_ref, normed_ref, out_ref):
+def dispatch_kernel(at_ref, target_ref, input_ref, gain_ref, out_ref):
     rows = out_ref.shape[0]
-    tokens = normed_ref.shape[0]
+    tokens, features = input_ref.shape
+    share = features // N_TP
+    own = pl.ds(pl.multiple_of(at_ref[1] * share, share), share)
+    squares = jnp.zeros((tokens, share), jnp.float32)
+    for k in range(N_TP):
+        part = input_ref[:, k * share : (k + 1) * share].astype(jnp.float32)
+        squares = squares + part * part
+    scale = lax.rsqrt(jnp.sum(squares, axis=1, keepdims=True) * (1.0 / features) + EPS)
+    normed = (input_ref[:, own].astype(jnp.float32) * scale * gain_ref[:, own]).astype(jnp.bfloat16)
     row = lax.broadcasted_iota(jnp.int32, (rows, tokens), 0)
     place = row % 8
-    first = (row // 8) * 16 + chunk_ref[0] * SLOTS
+    first = (row // 8) * 16 + at_ref[0] * SLOTS
 
     def picks(slot):
         hit = target_ref[0:1, :] == slot
@@ -52,24 +60,24 @@
         return jnp.where(hit, 1.0, 0.0).astype(jnp.bfloat16)
 
     main = picks(jnp.where(place < SLOTS, first + place, -1))
-    last = normed_ref[:, BLOCKS * LANES :]
+    last = normed[:, BLOCKS * LANES :]
     for b in range(BLOCKS):
         extra = picks(jnp.where(place < SLOTS, -1, first + 2 * b + place - SLOTS))
         cols = slice(b * LANES, (b + 1) * LANES)
-        out_ref[:, cols] = (dot(main, normed_ref[:, cols]) + dot(extra, last)).astype(out_ref.dtype)
-
-
-def dispatched(chunk, target, normed, rows):
+        out_ref[:, cols] = (dot(main, normed[:, cols]) + dot(extra, last)).astype(out_ref.dtype)
+
+
+def dispatched(chunk, tp, target, tokens, gain, rows):
     vmem = pl.BlockSpec(memory_space=pltpu.VMEM)
     return pl.pallas_call(
         dispatch_kernel,
-        in_specs=[pl.BlockSpec(memory_space=pltpu.SMEM), vmem, vmem],
+        in_specs=[pl.BlockSpec(memory_space=pltpu.SMEM), vmem, vmem, vmem],
         out_specs=vmem,
         out_shape=jax.ShapeDtypeStruct((rows, BLOCKS * LANES), jnp.bfloat16),
-        compiler_params=params(12),
+        compiler_params=params(56),
         cost_estimate=cost(4 * rows * 128 * 768, 1 << 20),
         name="dispatch",
-    )(jnp.full((1,), chunk, jnp.int32), target, normed)
+    )(jnp.stack([jnp.int32(chunk), tp]), target, tokens, gain)
 
 
 def hidden_kernel(tp_ref, own, nt, nb, ft, fb, pt, pb, gate_ref, up_ref, out_ref, held, acc, sems):
@@ -321,14 +329,12 @@
     rank = jnp.sum(same.astype(jnp.int32), axis=0)
     target = (ids * 16 + rank).reshape(TOPK, token_rows)
 
-    widened = expert_input.astype(jnp.float32)
-    scale = lax.rsqrt(jnp.mean(widened * widened, axis=-1, keepdims=True) + EPS)
-    own = lax.dynamic_slice_in_dim(expert_input, tp * share, share, 1).astype(jnp.float32)
-    gain = lax.dynamic_slice_in_dim(norm_gain, tp * share, share, 0)
-    normed = (own * scale * gain[None, :]).astype(bf)
-
-    got1 = exchanged(dispatched(0, target, normed, experts * 8))
-    got2 = exchanged(dispatched(1, target, normed, experts * 8))
+    gain = norm_gain[None, :]
+    tp_index = tp.astype(jnp.int32)
+    sent1 = dispatched(0, tp_index, target, expert_input, gain, experts * 8)
+    got1 = exchanged(sent1)
+    sent2 = dispatched(1, tp_index, target, expert_input, gain, experts * 8)
+    got2 = exchanged(sent2)
 
     downs = []
     for k in range(N_TP):

time: 237 us -> 236 us (level)
  Pallas kernels: 26.6 us -> 29.6 us
    pallas_call x2, Pallas kernels: 3.29 us -> 6.29 us  [dispatched(): pl.pallas_call(dispatch_kernel, in_specs=[pl.BlockSpec(memory_space=pltpu...]
  transfers between devices with their start and end apart: 29 -> 29, of which waited for: 18 -> 18; matrix products, arithmetic and copies ran while one was open for 5% -> 5% of each run, Pallas kernels for 10% -> 11%
where the time goes in v2:
time: 236 us; the launch traced here: 234 us
  waiting for transfers between devices  111 us (47%)
  starting transfers between devices  75.9 us (32%)
  Pallas kernels  29.6 us (13%)
  local copies, waits for them, and re-layouts  9.38 us (4%)
  other arithmetic  3.96 us (2%)
  matrix products  3.45 us (1%)
    ppermute x24, waiting for transfers between devices, shifted(): lax.ppermute(block, 'tp', [((i + distance) % N_TP, i) for i in range(N_TP)])  72.7 us
    all_to_all x4, starting transfers between devices, exchanged(): return lax.all_to_all(block, 'ep', split_axis=0, concat_axis=0, tiled=True)  38.7 us
    all_to_all x4, waiting for transfers between devices, exchanged(): return lax.all_to_all(block, 'ep', split_axis=0, concat_axis=0, tiled=True)  38.2 us
    ppermute x24, starting transfers between devices, shifted(): lax.ppermute(block, 'tp', [((i + distance) % N_TP, i) for i in range(N_TP)])  35.3 us
    pallas_call x2, Pallas kernels, hidden(): pl.pallas_call(hidden_kernel, grid_spec=pltpu.PrefetchScalarGridSpec(num_...  13.6 us
    pallas_call x2, Pallas kernels, dispatched(): pl.pallas_call(dispatch_kernel, in_specs=[pl.BlockSpec(memory_space=pltpu...  6.29 us
  transfers between devices with their start and end apart: 29, of which 18 were waited for; matrix products, arithmetic and copies ran while one was open for 5% of the time, Pallas kernels for 11%

profile of v2, /device:TPU:2, one launch (start us, length us, event | category | flops | bytes accessed | tf_op | source)
XLA Modules:
  0.0 234.1 jit_solution(17655322923920589734)
XLA Ops:
  3.0 3.1 %dispatch.3 = bf16[512,768]{1,0:T(8,128)(2,1)} custom-call(s32[2]{0:T(128)} %pad_add_fusion.1.at_ref, s32[4,128]{1,0:T(4,128)} %copy.37.target_ref, bf16[128,4096]{1,0:T(8,128)(2,1)} %input_ref.3, f32[1,4096]{1,0:T(1,128)} %bitcast.48), custom_call_target="tpu_custom_call" | custom-call | flops 201326592 | bytes 1048576 | tf_op jit(solution)/shard_map/dispatch/pallas_call | solution.py:72
  6.2 12.0 %all-to-all-start.2 = ((bf16[64,8,768]{2,1,0:T(8,128)(2,1)}), bf16[64,8,768]{2,1,0:T(8,128)(2,1)S(1)}, u32[]{:S(2)}, u32[]{:S(2)}) async-start(bf16[64,8,768]{2,1,0:T(8,128)(2,1)} %bitcast.46), calls=%async_computation.2 | async-start | bytes 1572864 | tf_op jit(solution)/shard_map/all_to_all | solution.py:26
  18.8 3.2 %dispatch.2 = bf16[512,768]{1,0:T(8,128)(2,1)} custom-call(s32[2]{0:T(128)} %pad_add_fusion.at_ref, s32[4,128]{1,0:T(4,128)} %copy.37.target_ref, bf16[128,4096]{1,0:T(8,128)(2,1)} %input_ref.3, f32[1,4096]{1,0:T(1,128)} %bitcast.49), custom_call_target="tpu_custom_call" | custom-call | flops 201326592 | bytes 1048576 | tf_op jit(solution)/shard_map/dispatch/pallas_call | solution.py:72
  22.0 19.4 %all-to-all-done.2 = bf16[64,8,768]{2,1,0:T(8,128)(2,1)S(1)} async-done(((bf16[64,8,768]{2,1,0:T(8,128)(2,1)}), bf16[64,8,768]{2,1,0:T(8,128)(2,1)S(1)}, u32[]{:S(2)}, u32[]{:S(2)}) %all-to-all-start.2) | async-done | bytes 786464 | tf_op jit(solution)/shard_map/all_to_all | solution.py:26
  41.4 5.9 %all-to-all-start = ((bf16[64,8,768]{2,1,0:T(8,128)(2,1)}), bf16[64,8,768]{2,1,0:T(8,128)(2,1)}, u32[]{:S(2)}, u32[]{:S(2)}) async-start(bf16[64,8,768]{2,1,0:T(8,128)(2,1)} %bitcast.45), calls=%async_computation | async-start | bytes 1572864 | tf_op jit(solution)/shard_map/all_to_all | solution.py:26
  47.4 3.1 %collective-permute-start.16 = (bf16[256,768]{1,0:T(8,128)(2,1)S(1)}, bf16[256,768]{1,0:T(8,128)(2,1)S(1)}, u32[]{:S(2)}, u32[]{:S(2)}) collective-permute-start(bf16[256,768]{1,0:T(8,128)(2,1)S(1)} %get-tuple-element.14), channel_id=1, source_target_pairs={{1,0},{2,1},{3,2},{0,3},{5,4},{6,5},{7,6},{4,7},{9,8},{10,9},{11,1... | collective-permute-start | bytes 1179656 | tf_op jit(solution)/shard_map/ppermute | solution.py:22
  50.4 3.2 %collective-permute-start.17 = (bf16[256,768]{1,0:T(8,128)(2,1)S(1)}, bf16[256,768]{1,0:T(8,128)(2,1)}, u32[]{:S(2)}, u32[]{:S(2)}) collective-permute-start(bf16[256,768]{1,0:T(8,128)(2,1)S(1)} %get-tuple-element.13), channel_id=1, source_target_pairs={{1,0},{2,1},{3,2},{0,3},{5,4},{6,5},{7,6},{4,7},{9,8},{10,9},{11,1... | collective-permute-start | bytes 1179656 | tf_op jit(solution)/shard_map/ppermute | solution.py:22
  55.4 3.3 %collective-permute-start.13 = (bf16[256,1024]{1,0:T(8,128)(2,1)S(1)}, bf16[256,1024]{1,0:T(8,128)(2,1)S(1)}, u32[]{:S(2)}, u32[]{:S(2)}) collective-permute-start(bf16[256,1024]{1,0:T(8,128)(2,1)S(1)} %get-tuple-element.7), channel_id=1, source_target_pairs={{1,0},{2,1},{3,2},{0,3},{5,4},{6,5},{7,6},{4,7},{9,8},{10,9},{11,1... | collective-permute-start | bytes 1572872 | tf_op jit(solution)/shard_map/ppermute | solution.py:22
  60.0 3.7 %collective-permute-start.18 = (bf16[256,768]{1,0:T(8,128)(2,1)S(1)}, bf16[256,768]{1,0:T(8,128)(2,1)S(1)}, u32[]{:S(2)}, u32[]{:S(2)}) collective-permute-start(bf16[256,768]{1,0:T(8,128)(2,1)S(1)} %collective-permute-done.16.nt), channel_id=1, source_target_pairs={{1,0},{2,1},{3,2},{0,3},{5,4},{6,5},{7,6},{4,7},{9,8},{10,9},{11,1... | collective-permute-start | bytes 1179656 | tf_op jit(solution)/shard_map/ppermute | solution.py:22
  63.8 4.6 %collective-permute-done.17.nb = bf16[256,768]{1,0:T(8,128)(2,1)} collective-permute-done((bf16[256,768]{1,0:T(8,128)(2,1)S(1)}, bf16[256,768]{1,0:T(8,128)(2,1)}, u32[]{:S(2)}, u32[]{:S(2)}) %collective-permute-start.17) | collective-permute-done | bytes 393248 | tf_op jit(solution)/shard_map/ppermute | solution.py:22
  68.4 2.8 %collective-permute-start.14 = (bf16[256,1024]{1,0:T(8,128)(2,1)S(1)}, bf16[256,1024]{1,0:T(8,128)(2,1)S(1)}, u32[]{:S(2)}, u32[]{:S(2)}) collective-permute-start(bf16[256,1024]{1,0:T(8,128)(2,1)S(1)} %get-tuple-element.9), channel_id=1, source_target_pairs={{2,0},{3,1},{0,2},{1,3},{6,4},{7,5},{4,6},{5,7},{10,8},{11,9},{8,1... | collective-permute-start | bytes 1572872 | tf_op jit(solution)/shard_map/ppermute | solution.py:22
  73.0 25.4 %collective-permute-done.18.ft = bf16[256,768]{1,0:T(8,128)(2,1)S(1)} collective-permute-done((bf16[256,768]{1,0:T(8,128)(2,1)S(1)}, bf16[256,768]{1,0:T(8,128)(2,1)S(1)}, u32[]{:S(2)}, u32[]{:S(2)}) %collective-permute-start.18) | collective-permute-done | bytes 393248 | tf_op jit(solution)/shard_map/ppermute | solution.py:22
  99.3 6.8 %hidden.3.a0 = bf16[384,256]{1,0:T(8,128)(2,1)} custom-call(s32[1]{0:T(128)} %bitcast.5.tp_ref, bf16[512,768]{1,0:T(8,128)(2,1)} %bitcast.44, bf16[256,768]{1,0:T(8,128)(2,1)} %copy-done.8, bf16[256,768]{1,0:T(8,128)(2,1)} %collective-permute-done.17.nb, bf16[256,768]{1,0:T(8,128)(2,1)} %copy-done.12, bf16[256,768]{1,0:T(8,128)(2,1)} %copy-done.14, ...), custom_call_target="tpu_custom_call" | custom-call | flops 805306368 | bytes 8388608 | tf_op jit(solution)/shard_map/hidden/pallas_call | solution.py:145
  106.1 3.8 %collective-permute-start.22 = (bf16[384,256]{1,0:T(8,128)(2,1)}, bf16[384,256]{1,0:T(8,128)(2,1)S(1)}, u32[]{:S(2)}, u32[]{:S(2)}) collective-permute-start(bf16[384,256]{1,0:T(8,128)(2,1)} %hidden.3.a0), channel_id=1, source_target_pairs={{1,0},{2,1},{3,2},{0,3},{5,4},{6,5},{7,6},{4,7},{9,8},{10,9},{11,1... | collective-permute-start | bytes 589832 | tf_op jit(solution)/shard_map/ppermute | solution.py:22
  110.9 7.1 %collective-permute-done.22.a1 = bf16[384,256]{1,0:T(8,128)(2,1)S(1)} collective-permute-done((bf16[384,256]{1,0:T(8,128)(2,1)}, bf16[384,256]{1,0:T(8,128)(2,1)S(1)}, u32[]{:S(2)}, u32[]{:S(2)}) %collective-permute-start.22) | collective-permute-done | bytes 196640 | tf_op jit(solution)/shard_map/ppermute | solution.py:22
  124.3 10.5 %all-to-all-start.3 = ((bf16[64,8,768]{2,1,0:T(8,128)(2,1)}), bf16[64,8,768]{2,1,0:T(8,128)(2,1)S(1)}, u32[]{:S(2)}, u32[]{:S(2)}) async-start(bf16[64,8,768]{2,1,0:T(8,128)(2,1)} %bitcast.23), calls=%async_computation.3 | async-start | bytes 1572864 | tf_op jit(solution)/shard_map/all_to_all | solution.py:26
  143.0 6.1 %collective-permute-done.4.nt = bf16[256,768]{1,0:T(8,128)(2,1)} collective-permute-done((bf16[256,768]{1,0:T(8,128)(2,1)}, bf16[256,768]{1,0:T(8,128)(2,1)}, u32[]{:S(2)}, u32[]{:S(2)}) %collective-permute-start.4) | collective-permute-done | bytes 393248 | tf_op jit(solution)/shard_map/ppermute | solution.py:22
  153.6 3.4 %convolution_convert_fusion = bf16[256,4096]{1,0:T(8,128)(2,1)S(1)} fusion(bf16[256,512]{1,0:T(8,128)(2,1)S(1)} %attention.1, bf16[512,4096]{1,0:T(8,128)(2,1)} %param.16), kind=kOutput, calls=%fused_computation | convolution fusion | flops 1074790400 | bytes 6553600 | tf_op jit(solution)/shard_map/dot_general | solution.py:30
  159.5 5.5 %collective-permute-done.6.ft = bf16[256,768]{1,0:T(8,128)(2,1)S(1)} collective-permute-done((bf16[256,768]{1,0:T(8,128)(2,1)}, bf16[256,768]{1,0:T(8,128)(2,1)S(1)}, u32[]{:S(2)}, u32[]{:S(2)}) %collective-permute-start.6) | collective-permute-done | bytes 393248 | tf_op jit(solution)/shard_map/ppermute | solution.py:22
  167.6 6.8 %hidden.2.a0 = bf16[384,256]{1,0:T(8,128)(2,1)} custom-call(s32[1]{0:T(128)} %bitcast.5.tp_ref, bf16[512,768]{1,0:T(8,128)(2,1)} %bitcast.8.own, bf16[256,768]{1,0:T(8,128)(2,1)} %collective-permute-done.4.nt, bf16[256,768]{1,0:T(8,128)(2,1)} %copy-done.9, bf16[256,768]{1,0:T(8,128)(2,1)} %copy-done.11, bf16[256,768]{1,0:T(8,128)(2,1)} %copy-done.13, ...), custom_call_target="tpu_custom_call" | custom-call | flops 805306368 | bytes 8388608 | tf_op jit(solution)/shard_map/hidden/pallas_call | solution.py:145
  177.6 3.2 %collective-permute-start.1 = (bf16[64,4096]{1,0:T(8,128)(2,1)}, bf16[64,4096]{1,0:T(8,128)(2,1)}, u32[]{:S(2)}, u32[]{:S(2)}) collective-permute-start(bf16[64,4096]{1,0:T(8,128)(2,1)} %get-tuple-element.10), channel_id=1, source_target_pairs={{1,0},{2,1},{3,2},{0,3},{5,4},{6,5},{7,6},{4,7},{9,8},{10,9},{11,1... | collective-permute-start | bytes 1572872 | tf_op jit(solution)/shard_map/ppermute | solution.py:22
  184.4 12.5 %collective-permute-done.12.a3 = bf16[384,256]{1,0:T(8,128)(2,1)S(1)} collective-permute-done((bf16[384,256]{1,0:T(8,128)(2,1)}, bf16[384,256]{1,0:T(8,128)(2,1)S(1)}, u32[]{:S(2)}, u32[]{:S(2)}) %collective-permute-start.12) | collective-permute-done | bytes 196640 | tf_op jit(solution)/shard_map/ppermute | solution.py:22
  198.8 10.3 %all-to-all-start.1 = ((bf16[64,8,768]{2,1,0:T(8,128)(2,1)}), bf16[64,8,768]{2,1,0:T(8,128)(2,1)S(1)}, u32[]{:S(2)}, u32[]{:S(2)}) async-start(bf16[64,8,768]{2,1,0:T(8,128)(2,1)} %bitcast.17), calls=%async_computation.1 | async-start | bytes 1572864 | tf_op jit(solution)/shard_map/all_to_all | solution.py:26
  213.6 18.7 %all-to-all-done.1 = bf16[64,8,768]{2,1,0:T(8,128)(2,1)S(1)} async-done(((bf16[64,8,768]{2,1,0:T(8,128)(2,1)}), bf16[64,8,768]{2,1,0:T(8,128)(2,1)S(1)}, u32[]{:S(2)}, u32[]{:S(2)}) %all-to-all-start.1) | async-done | bytes 786464 | tf_op jit(solution)/shard_map/all_to_all | solution.py:26
  (96 shorter events, 48.7 us)
Async XLA Ops:
  6.2 35.2 %all-to-all-start.2 = ((bf16[64,8,768]{2,1,0:T(8,128)(2,1)}), bf16[64,8,768]{2,1,0:T(8,128)(2,1)S(1)}, u32[]{:S(2)}, u32[]{:S(2)}) async-start(bf16[64,8,768]{2,1,0:T(8,128)(2,1)} %bitcast.46), calls=%async_computation.2 | async-start | bytes 1572864 | tf_op jit(solution)/shard_map/all_to_all | solution.py:26
  41.4 82.9 %all-to-all-start = ((bf16[64,8,768]{2,1,0:T(8,128)(2,1)}), bf16[64,8,768]{2,1,0:T(8,128)(2,1)}, u32[]{:S(2)}, u32[]{:S(2)}) async-start(bf16[64,8,768]{2,1,0:T(8,128)(2,1)} %bitcast.45), calls=%async_computation | async-start | bytes 1572864 | tf_op jit(solution)/shard_map/all_to_all | solution.py:26
  47.4 12.6 %collective-permute-start.16 = (bf16[256,768]{1,0:T(8,128)(2,1)S(1)}, bf16[256,768]{1,0:T(8,128)(2,1)S(1)}, u32[]{:S(2)}, u32[]{:S(2)}) collective-permute-start(bf16[256,768]{1,0:T(8,128)(2,1)S(1)} %get-tuple-element.14), channel_id=1, source_target_pairs={{1,0},{2,1},{3,2},{0,3},{5,4},{6,5},{7,6},{4,7},{9,8},{10,9},{11,1... | collective-permute-start | bytes 1179656 | tf_op jit(solution)/shard_map/ppermute | solution.py:22
  50.4 13.3 %collective-permute-start.19 = (bf16[256,768]{1,0:T(8,128)(2,1)S(1)}, bf16[256,768]{1,0:T(8,128)(2,1)}, u32[]{:S(2)}, u32[]{:S(2)}) collective-permute-start(bf16[256,768]{1,0:T(8,128)(2,1)S(1)} %get-tuple-element.13), channel_id=1, source_target_pairs={{3,0},{0,1},{1,2},{2,3},{7,4},{4,5},{5,6},{6,7},{11,8},{8,9},{9,10... | collective-permute-start | bytes 1179656 | tf_op jit(solution)/shard_map/ppermute | solution.py:22
  50.4 17.9 %collective-permute-start.17 = (bf16[256,768]{1,0:T(8,128)(2,1)S(1)}, bf16[256,768]{1,0:T(8,128)(2,1)}, u32[]{:S(2)}, u32[]{:S(2)}) collective-permute-start(bf16[256,768]{1,0:T(8,128)(2,1)S(1)} %get-tuple-element.13), channel_id=1, source_target_pairs={{1,0},{2,1},{3,2},{0,3},{5,4},{6,5},{7,6},{4,7},{9,8},{10,9},{11,1... | collective-permute-start | bytes 1179656 | tf_op jit(solution)/shard_map/ppermute | solution.py:22
  53.7 18.5 %collective-permute-start.21 = (bf16[256,768]{1,0:T(8,128)(2,1)S(1)}, bf16[256,768]{1,0:T(8,128)(2,1)}, u32[]{:S(2)}, u32[]{:S(2)}) collective-permute-start(bf16[256,768]{1,0:T(8,128)(2,1)S(1)} %get-tuple-element.14), channel_id=1, source_target_pairs={{3,0},{0,1},{1,2},{2,3},{7,4},{4,5},{5,6},{6,7},{11,8},{8,9},{9,10... | collective-permute-start | bytes 1179656 | tf_op jit(solution)/shard_map/ppermute | solution.py:22
  55.4 54.5 %collective-permute-start.13 = (bf16[256,1024]{1,0:T(8,128)(2,1)S(1)}, bf16[256,1024]{1,0:T(8,128)(2,1)S(1)}, u32[]{:S(2)}, u32[]{:S(2)}) collective-permute-start(bf16[256,1024]{1,0:T(8,128)(2,1)S(1)} %get-tuple-element.7), channel_id=1, source_target_pairs={{1,0},{2,1},{3,2},{0,3},{5,4},{6,5},{7,6},{4,7},{9,8},{10,9},{11,1... | collective-permute-start | bytes 1572872 | tf_op jit(solution)/shard_map/ppermute | solution.py:22
  60.0 38.5 %collective-permute-start.18 = (bf16[256,768]{1,0:T(8,128)(2,1)S(1)}, bf16[256,768]{1,0:T(8,128)(2,1)S(1)}, u32[]{:S(2)}, u32[]{:S(2)}) collective-permute-start(bf16[256,768]{1,0:T(8,128)(2,1)S(1)} %collective-permute-done.16.nt), channel_id=1, source_target_pairs={{1,0},{2,1},{3,2},{0,3},{5,4},{6,5},{7,6},{4,7},{9,8},{10,9},{11,1... | collective-permute-start | bytes 1179656 | tf_op jit(solution)/shard_map/ppermute | solution.py:22
  63.7 34.7 %collective-permute-start.20 = (bf16[256,768]{1,0:T(8,128)(2,1)}, bf16[256,768]{1,0:T(8,128)(2,1)S(1)}, u32[]{:S(2)}, u32[]{:S(2)}) collective-permute-start(bf16[256,768]{1,0:T(8,128)(2,1)} %collective-permute-done.19.pb), channel_id=1, source_target_pairs={{3,0},{0,1},{1,2},{2,3},{7,4},{4,5},{5,6},{6,7},{11,8},{8,9},{9,10... | collective-permute-start | bytes 1179656 | tf_op jit(solution)/shard_map/ppermute | solution.py:22
  68.4 42.5 %collective-permute-start.14 = (bf16[256,1024]{1,0:T(8,128)(2,1)S(1)}, bf16[256,1024]{1,0:T(8,128)(2,1)S(1)}, u32[]{:S(2)}, u32[]{:S(2)}) collective-permute-start(bf16[256,1024]{1,0:T(8,128)(2,1)S(1)} %get-tuple-element.9), channel_id=1, source_target_pairs={{2,0},{3,1},{0,2},{1,3},{6,4},{7,5},{4,6},{5,7},{10,8},{11,9},{8,1... | collective-permute-start | bytes 1572872 | tf_op jit(solution)/shard_map/ppermute | solution.py:22
  72.2 38.7 %collective-permute-start.15 = (bf16[256,1024]{1,0:T(8,128)(2,1)S(1)}, bf16[256,1024]{1,0:T(8,128)(2,1)S(1)}, u32[]{:S(2)}, u32[]{:S(2)}) collective-permute-start(bf16[256,1024]{1,0:T(8,128)(2,1)S(1)} %get-tuple-element.6), channel_id=1, source_target_pairs={{3,0},{0,1},{1,2},{2,3},{7,4},{4,5},{5,6},{6,7},{11,8},{8,9},{9,10... | collective-permute-start | bytes 1572872 | tf_op jit(solution)/shard_map/ppermute | solution.py:22
  124.3 74.6 %all-to-all-start.3 = ((bf16[64,8,768]{2,1,0:T(8,128)(2,1)}), bf16[64,8,768]{2,1,0:T(8,128)(2,1)S(1)}, u32[]{:S(2)}, u32[]{:S(2)}) async-start(bf16[64,8,768]{2,1,0:T(8,128)(2,1)} %bitcast.23), calls=%async_computation.3 | async-start | bytes 1572864 | tf_op jit(solution)/shard_map/all_to_all | solution.py:26
  136.8 12.3 %collective-permute-start.4 = (bf16[256,768]{1,0:T(8,128)(2,1)}, bf16[256,768]{1,0:T(8,128)(2,1)}, u32[]{:S(2)}, u32[]{:S(2)}) collective-permute-start(bf16[256,768]{1,0:T(8,128)(2,1)} %get-tuple-element.16), channel_id=1, source_target_pairs={{1,0},{2,1},{3,2},{0,3},{5,4},{6,5},{7,6},{4,7},{9,8},{10,9},{11,1... | collective-permute-start | bytes 1179656 | tf_op jit(solution)/shard_map/ppermute | solution.py:22
  137.7 13.5 %collective-permute-start.7 = (bf16[256,768]{1,0:T(8,128)(2,1)}, bf16[256,768]{1,0:T(8,128)(2,1)}, u32[]{:S(2)}, u32[]{:S(2)}) collective-permute-start(bf16[256,768]{1,0:T(8,128)(2,1)} %get-tuple-element.15), channel_id=1, source_target_pairs={{3,0},{0,1},{1,2},{2,3},{7,4},{4,5},{5,6},{6,7},{11,8},{8,9},{9,10... | collective-permute-start | bytes 1179656 | tf_op jit(solution)/shard_map/ppermute | solution.py:22
  138.8 12.4 %collective-permute-start = (bf16[128,256]{1,0:T(8,128)(2,1)S(1)}, bf16[128,256]{1,0:T(8,128)(2,1)S(1)}, u32[]{:S(2)}, u32[]{:S(2)}) collective-permute-start(bf16[128,256]{1,0:T(8,128)(2,1)S(1)} %pad_maximum_fusion), channel_id=1, source_target_pairs={{0,4},{4,8},{8,12},{12,16},{16,20},{20,24},{24,28},{28,32},{32,36}... | collective-permute-start | bytes 196616 | tf_op jit(solution)/shard_map/ppermute | solution.py:243
  140.8 16.6 %collective-permute-start.5 = (bf16[256,768]{1,0:T(8,128)(2,1)}, bf16[256,768]{1,0:T(8,128)(2,1)S(1)}, u32[]{:S(2)}, u32[]{:S(2)}) collective-permute-start(bf16[256,768]{1,0:T(8,128)(2,1)} %get-tuple-element.15), channel_id=1, source_target_pairs={{1,0},{2,1},{3,2},{0,3},{5,4},{6,5},{7,6},{4,7},{9,8},{10,9},{11,1... | collective-permute-start | bytes 1179656 | tf_op jit(solution)/shard_map/ppermute | solution.py:22
  143.0 16.5 %collective-permute-start.9 = (bf16[256,768]{1,0:T(8,128)(2,1)}, bf16[256,768]{1,0:T(8,128)(2,1)S(1)}, u32[]{:S(2)}, u32[]{:S(2)}) collective-permute-start(bf16[256,768]{1,0:T(8,128)(2,1)} %get-tuple-element.16), channel_id=1, source_target_pairs={{3,0},{0,1},{1,2},{2,3},{7,4},{4,5},{5,6},{6,7},{11,8},{8,9},{9,10... | collective-permute-start | bytes 1179656 | tf_op jit(solution)/shard_map/ppermute | solution.py:22
  149.1 15.9 %collective-permute-start.6 = (bf16[256,768]{1,0:T(8,128)(2,1)}, bf16[256,768]{1,0:T(8,128)(2,1)S(1)}, u32[]{:S(2)}, u32[]{:S(2)}) collective-permute-start(bf16[256,768]{1,0:T(8,128)(2,1)} %collective-permute-done.4.nt), channel_id=1, source_target_pairs={{1,0},{2,1},{3,2},{0,3},{5,4},{6,5},{7,6},{4,7},{9,8},{10,9},{11,1... | collective-permute-start | bytes 1179656 | tf_op jit(solution)/shard_map/ppermute | solution.py:22
  151.2 15.6 %collective-permute-start.8 = (bf16[256,768]{1,0:T(8,128)(2,1)}, bf16[256,768]{1,0:T(8,128)(2,1)S(1)}, u32[]{:S(2)}, u32[]{:S(2)}) collective-permute-start(bf16[256,768]{1,0:T(8,128)(2,1)} %collective-permute-done.7.pb), channel_id=1, source_target_pairs={{3,0},{0,1},{1,2},{2,3},{7,4},{4,5},{5,6},{6,7},{11,8},{8,9},{9,10... | collective-permute-start | bytes 1179656 | tf_op jit(solution)/shard_map/ppermute | solution.py:22
  176.4 20.4 %collective-permute-start.12 = (bf16[384,256]{1,0:T(8,128)(2,1)}, bf16[384,256]{1,0:T(8,128)(2,1)S(1)}, u32[]{:S(2)}, u32[]{:S(2)}) collective-permute-start(bf16[384,256]{1,0:T(8,128)(2,1)} %hidden.2.a0), channel_id=1, source_target_pairs={{3,0},{0,1},{1,2},{2,3},{7,4},{4,5},{5,6},{6,7},{11,8},{8,9},{9,10... | collective-permute-start | bytes 589832 | tf_op jit(solution)/shard_map/ppermute | solution.py:22
  177.6 31.7 %collective-permute-start.1 = (bf16[64,4096]{1,0:T(8,128)(2,1)}, bf16[64,4096]{1,0:T(8,128)(2,1)}, u32[]{:S(2)}, u32[]{:S(2)}) collective-permute-start(bf16[64,4096]{1,0:T(8,128)(2,1)} %get-tuple-element.10), channel_id=1, source_target_pairs={{1,0},{2,1},{3,2},{0,3},{5,4},{6,5},{7,6},{4,7},{9,8},{10,9},{11,1... | collective-permute-start | bytes 1572872 | tf_op jit(solution)/shard_map/ppermute | solution.py:22
  180.8 28.5 %collective-permute-start.2 = (bf16[64,4096]{1,0:T(8,128)(2,1)}, bf16[64,4096]{1,0:T(8,128)(2,1)}, u32[]{:S(2)}, u32[]{:S(2)}) collective-permute-start(bf16[64,4096]{1,0:T(8,128)(2,1)} %get-tuple-element.12), channel_id=1, source_target_pairs={{2,0},{3,1},{0,2},{1,3},{6,4},{7,5},{4,6},{5,7},{10,8},{11,9},{8,1... | collective-permute-start | bytes 1572872 | tf_op jit(solution)/shard_map/ppermute | solution.py:22
  182.4 26.9 %collective-permute-start.3 = (bf16[64,4096]{1,0:T(8,128)(2,1)S(1)}, bf16[64,4096]{1,0:T(8,128)(2,1)}, u32[]{:S(2)}, u32[]{:S(2)}) collective-permute-start(bf16[64,4096]{1,0:T(8,128)(2,1)S(1)} %get-tuple-element.11), channel_id=1, source_target_pairs={{3,0},{0,1},{1,2},{2,3},{7,4},{4,5},{5,6},{6,7},{11,8},{8,9},{9,10... | collective-permute-start | bytes 1572872 | tf_op jit(solution)/shard_map/ppermute | solution.py:22
  198.8 33.5 %all-to-all-start.1 = ((bf16[64,8,768]{2,1,0:T(8,128)(2,1)}), bf16[64,8,768]{2,1,0:T(8,128)(2,1)S(1)}, u32[]{:S(2)}, u32[]{:S(2)}) async-start(bf16[64,8,768]{2,1,0:T(8,128)(2,1)} %bitcast.17), calls=%async_computation.1 | async-start | bytes 1572864 | tf_op jit(solution)/shard_map/all_to_all | solution.py:26
  (23 other events, 330.6 us)
